TPU v7x, 128 devices: a whole 4x4x4 slice. The times are simulated.
128 devices in a mesh: sp: 16 (over z, x), tp: 8 (over y, core).
Axes of the slice: x: 4, y: 4, z: 4, core: 2. Of those that a mesh axis runs over, the one named last changes fastest.
Arguments:
- a_lin: bfloat16 [16384, 1024], P('sp', 'tp'), may hold values from -6 to 6
- a_gate: bfloat16 [16384, 1024], P('sp', 'tp'), may hold values from -9 to 9
- conv_weight: bfloat16 [31, 1024], P(None, 'tp'), may hold values from -7 to 7
- ln_gain: bfloat16 [1024], P('tp'), may hold values from 0.099609375 to 1.8984375
- ln_bias: bfloat16 [1024], P('tp'), may hold values from -3 to 3
- proj_weight: bfloat16 [1024, 2048], replicated, may hold values from -0.1875 to 0.1875
- residual: bfloat16 [16384, 2048], P(('sp', 'tp')), may hold values from -6 to 6
- mix_gain: bfloat16 [2048], replicated, may hold values from 0.099609375 to 1.8984375
- ffn_gain: bfloat16 [2048], replicated, may hold values from 0.099609375 to 1.8984375
- routes: int32 [16384, 2], P(('sp', 'tp')), may hold values from 0 to 15, all different within a row; in each aligned block of 128 rows (0 to 127, 128 to 255, ...) at most 20 rows name the same one
- route_weights: float32 [16384, 2], P(('sp', 'tp')), may hold values from 0.1 to 1
- gate_weight: bfloat16 [16, 2048, 7168], P('sp', None, 'tp'), may hold values from -0.125 to 0.125
- up_weight: bfloat16 [16, 2048, 7168], P('sp', None, 'tp'), may hold values from -0.125 to 0.125
- down_weight: bfloat16 [16, 7168, 2048], P('sp', 'tp'), may hold values from -0.0625 to 0.0625
- out_gain: bfloat16 [2048], replicated, may hold values from 0.099609375 to 1.8984375
Outputs:
- layer_out: bfloat16 [16384, 2048], P(('sp', 'tp'))
Inputs may be any that keep to these rules, and one draw needn't show every extreme that they name: In the rows of one device (128 aligned rows) no expert is named by more than 20 routes, a bound that some block reaches; the entries of one row differ.
All inputs are finite; a program needn't handle non-finite values.
Results may differ from a plain program's by a relative error of at most 0.018.
Values may be sent and summed in bfloat16 or wider, within the bound.
A program may use at most 128 MiB of HBM per device.

v0:
```python
import jax
import jax.numpy as jnp
from jax import lax
from jax.sharding import PartitionSpec as P

D = 2048
D_A = 1024


def passed_along(value, axis, steps):
    count = lax.axis_size(axis)
    leading, last = (max(0, -steps), min(count, count - steps))
    return lax.ppermute(value, axis, [(source, source + steps) for source in range(leading, last)])


def copy_for_each(value, axis):
    copies = jnp.broadcast_to(value, (lax.axis_size(axis), *value.shape))
    return lax.all_to_all(copies, axis, split_axis=0, concat_axis=0, tiled=True)


def over_copies(value, axis):
    return copy_for_each(value, axis).sum(axis=0)


def together(arrays, axis):
    ends = [0]
    for a in arrays:
        ends.append(ends[-1] + a.size)
    subtotal = over_copies(jnp.concatenate([a.ravel() for a in arrays]), axis)
    return tuple((subtotal[b:e].reshape(a.shape) for a, b, e in zip(arrays, ends, ends[1:])))


def laid_out(blocks, dim):
    dims = list(blocks.shape[1:])
    dims[dim] *= blocks.shape[0]
    return jnp.moveaxis(blocks, 0, dim).reshape(dims)


def work_in_pieces(value, axis, dim, work, out_dim):
    rows = value.shape[dim]
    pieces = jnp.split(value, 4, axis=dim) if rows % 4 == 0 else [value]
    leading = jnp.arange(lax.axis_size(axis)) * rows
    blocks = [lax.all_gather(piece, axis) for piece in pieces]
    made = [jax.vmap(work)(b, leading + k * (rows // len(pieces))) for k, b in enumerate(blocks)]
    return laid_out(jnp.concatenate(made, axis=out_dim + 1), out_dim)


def per_device(
    a_lin,
    a_gate,
    conv_weight,
    ln_gain,
    ln_bias,
    proj_weight,
    residual,
    mix_gain,
    ffn_gain,
    routes,
    route_weights,
    gate_weight,
    up_weight,
    down_weight,
    out_gain,
):
    kernel_len = conv_weight.shape[0]
    gated = (a_lin.astype(jnp.float32) * jax.nn.sigmoid(a_gate.astype(jnp.float32))).astype(
        jnp.bfloat16
    )
    row_count = gated.shape[0]
    edge_rows = passed_along(gated[row_count - (kernel_len - 1) :], "sp", 1)
    padded = jnp.concatenate([edge_rows, gated], 0).astype(jnp.float32)
    filter_taps = conv_weight.astype(jnp.float32)
    conv_out = filter_taps[0] * padded[0:row_count]
    for offset in range(1, kernel_len):
        conv_out = conv_out + filter_taps[offset] * padded[offset : offset + row_count]
    row_total, squares = together(
        (jnp.sum(conv_out, axis=1), jnp.sum(conv_out * conv_out, axis=1)), "tp"
    )
    row_mean = row_total / D_A
    row_var = squares / D_A - row_mean * row_mean
    scaled = (conv_out - row_mean[:, None]) * lax.rsqrt(row_var[:, None] + 1e-05)
    scaled = scaled * ln_gain.astype(jnp.float32) + ln_bias.astype(jnp.float32)
    activated = jax.nn.silu(scaled).astype(jnp.bfloat16)
    token_acts = lax.all_to_all(activated, "tp", split_axis=0, concat_axis=1, tiled=True)
    branch = jnp.dot(token_acts, proj_weight, preferred_element_type=jnp.float32)
    branch_f = lax.optimization_barrier(branch.astype(jnp.bfloat16)).astype(jnp.float32)
    branch_scale = lax.rsqrt(jnp.mean(branch_f * branch_f, axis=1, keepdims=True) + 1e-06)
    stream = residual.astype(jnp.float32) + branch_f * branch_scale * mix_gain.astype(jnp.float32)
    stream_scale = lax.rsqrt(jnp.mean(stream * stream, axis=1, keepdims=True) + 1e-06)
    normed = (stream * stream_scale * ffn_gain.astype(jnp.float32)).astype(jnp.bfloat16)
    tok_count = routes.shape[0]
    top_count = routes.shape[1]
    experts = lax.axis_size("sp")
    capacity = max(2, 5 * tok_count * top_count // (4 * experts))
    flat_routes = routes.reshape(-1)
    matches = (flat_routes[:, None] == jnp.arange(experts, dtype=jnp.int32)[None, :]).astype(
        jnp.int32
    )
    before = jnp.cumsum(matches, axis=0) - matches
    slot_index = jnp.sum(before * matches, axis=1)
    target = flat_routes * capacity + slot_index
    target_hit = (
        target.reshape(tok_count, top_count)[None, :, :]
        == jnp.arange(experts * capacity, dtype=jnp.int32)[:, None, None]
    )
    dispatch = jnp.any(target_hit, axis=2).astype(jnp.bfloat16)
    outgoing = jnp.dot(dispatch, normed, preferred_element_type=jnp.float32).astype(jnp.bfloat16)
    outgoing = outgoing.reshape(experts, capacity, D)
    w_gate = gate_weight[0]
    w_up = up_weight[0]
    w_down = down_weight[0]

    def expert_terms(block_rows, first_index):
        piece_dims = block_rows.shape
        flat_rows = block_rows.reshape(-1, piece_dims[-1])
        gate_proj = jnp.dot(flat_rows, w_gate, preferred_element_type=jnp.float32)
        up_proj = jnp.dot(flat_rows, w_up, preferred_element_type=jnp.float32)
        hidden = (jax.nn.silu(gate_proj) * up_proj).astype(jnp.bfloat16)
        return jnp.dot(hidden, w_down, preferred_element_type=jnp.float32).reshape(piece_dims)

    arrived = lax.all_to_all(outgoing, "sp", split_axis=0, concat_axis=0, tiled=True)
    partials = work_in_pieces(arrived[:, None], "tp", 1, expert_terms, 1)
    summed = lax.psum_scatter(partials.astype(jnp.bfloat16), "tp", scatter_dimension=1, tiled=True)
    own_results = summed.reshape(experts, capacity, D)
    returned = lax.all_to_all(own_results, "sp", split_axis=0, concat_axis=0, tiled=True)
    picked = returned.reshape(experts * capacity, D)[target]
    picked = picked.astype(jnp.float32).reshape(tok_count, top_count, D)
    expert_mix = jnp.sum(picked * route_weights[:, :, None], axis=1)
    mix_scale = lax.rsqrt(jnp.mean(expert_mix * expert_mix, axis=1, keepdims=True) + 1e-06)
    return (stream + expert_mix * mix_scale * out_gain.astype(jnp.float32)).astype(jnp.bfloat16)


def solution(mesh):
    return jax.shard_map(
        per_device,
        mesh=mesh,
        in_specs=(
            P("sp", "tp"),
            P("sp", "tp"),
            P(None, "tp"),
            P("tp"),
            P("tp"),
            P(),
            P(("sp", "tp"), None),
            P(),
            P(),
            P(("sp", "tp"), None),
            P(("sp", "tp"), None),
            P("sp", None, "tp"),
            P("sp", None, "tp"),
            P("sp", "tp", None),
            P(),
        ),
        out_specs=P(("sp", "tp"), None),
        check_vma=False,
    )
```

profile of v0, /device:TPU:0, one launch (start us, length us, event | category | flops | bytes accessed | tf_op | source)
XLA Modules:
  0.0 335.1 jit_solution(13111588587481648117)
XLA Ops:
  6.5 1.2 multiply_convert_fusion.4
  7.7 3.5 %collective-permute-start = (bf16[30,128]{1,0:T(8,128)(2,1)S(1)}, bf16[30,128]{1,0:T(8,128)(2,1)S(1)}, u32[]{:S(2)}, u32[]{:S(2)}) collective-permute-start(bf16[30,128]{1,0:T(8,128)(2,1)S(1)} %slice.271), channel_id=1, source_target_pairs={{0,8},{8,16},{16,24},{24,32},{32,40},{40,48},{48,56},{56,64},{64,7... | collective-permute-start | bytes 23048 | tf_op jit(solution)/shard_map/ppermute | solution.py:13
  11.2 0.7 convert_element_type.82
  12.0 0.8 copy.56
  12.8 0.1 eq.42
  12.9 0.6 reduce-window.6
  13.5 0.2 slice_reduce_fusion
  13.7 0.1 eq.38
  13.8 0.7 convert_element_type.87
  14.5 0.7 convert_element_type.88
  15.3 2.4 fusion.51
  17.7 0.7 broadcast_in_dim.2
  18.4 4.5 %all-to-all-start = ((f32[8,1,2048]{2,1,0:T(1,128)}), f32[8,1,2048]{2,1,0:T(1,128)S(1)}, u32[]{:S(2)}, u32[]{:S(2)}) async-start(f32[8,1,2048]{2,1,0:T(1,128)} %broadcast_in_dim.2), calls=%async_computation | async-start | bytes 131072 | tf_op jit(solution)/shard_map/all_to_all | solution.py:18
  22.8 0.1 fusion.45
  22.9 0.1 reduce_sum.81
  23.1 5.4 %all-to-all-done = f32[8,1,2048]{2,1,0:T(1,128)S(1)} async-done(((f32[8,1,2048]{2,1,0:T(1,128)}), f32[8,1,2048]{2,1,0:T(1,128)S(1)}, u32[]{:S(2)}, u32[]{:S(2)}) %all-to-all-start) | async-done | bytes 65568 | tf_op jit(solution)/shard_map/all_to_all | solution.py:18
  28.5 1.1 multiply_convert_fusion.3
  29.6 3.4 %all-to-all-start.1 = ((bf16[8,128,128]{2,1,0:T(8,128)(2,1)}), bf16[8,128,128]{2,1,0:T(8,128)(2,1)S(1)}, u32[]{:S(2)}, u32[]{:S(2)}) async-start(bf16[8,128,128]{2,1,0:T(8,128)(2,1)} %bitcast.31), calls=%async_computation.1 | async-start | bytes 524288 | tf_op jit(solution)/shard_map/all_to_all | solution.py:84
  33.1 0.1 copy.60
  33.2 0.1 fusion.42
  33.2 7.2 %all-to-all-done.1 = bf16[8,128,128]{2,1,0:T(8,128)(2,1)S(1)} async-done(((bf16[8,128,128]{2,1,0:T(8,128)(2,1)}), bf16[8,128,128]{2,1,0:T(8,128)(2,1)S(1)}, u32[]{:S(2)}, u32[]{:S(2)}) %all-to-all-start.1) | async-done | bytes 262176 | tf_op jit(solution)/shard_map/all_to_all | solution.py:84
  40.4 0.2 copy.55
  40.6 2.9 convolution_convert_fusion.1
  43.6 0.2 fusion.5
  43.8 0.4 multiply_reduce_fusion.2
  44.2 0.7 convolution_convert_fusion
  44.8 0.3 reshape.120
  45.2 29.8 %all_to_all.35 = bf16[16,20,2048]{2,1,0:T(8,128)(2,1)S(1)} all-to-all(bf16[16,20,2048]{2,1,0:T(8,128)(2,1)S(1)} %reshape.120), channel_id=1, replica_groups=mesh['sp'=16,'tp'=8] {'sp'}, dimensions={0} | all-to-all | bytes 2621440 | tf_op jit(solution)/shard_map/all_to_all | solution.py:121
  74.9 1.8 copy.61
  76.8 0.2 reduce-scatter.2.cloned.1.call-start
  77.0 54.0 %all-gather.3.cloned.1.call-done = bf16[128,20,2048]{2,0,1:T(8,128)(2,1)} async-done(((bf16[16,20,2048]{2,0,1:T(8,128)(2,1)}), bf16[128,20,2048]{2,0,1:T(8,128)(2,1)}) %all-gather.3.cloned.1.call-update) | async-done | bytes 10485776 | tf_op jit(solution)/shard_map/all_gather | solution.py:43
  131.0 14.0 %copy.62 = bf16[128,20,2048]{2,1,0:T(8,128)(2,1)} copy(bf16[128,20,2048]{2,0,1:T(8,128)(2,1)} %all-gather.3.cloned.1.call-done) | data formatting | bytes 20971520 | tf_op jit(solution)/shard_map/all_gather | solution.py:43
  145.0 16.5 %reshape.121 = bf16[8,320,2048]{2,1,0:T(8,128)(2,1)} reshape(bf16[128,20,2048]{2,1,0:T(8,128)(2,1)} %copy.62) | data formatting | bytes 20971520 | tf_op jit(solution)/shard_map/vmap()/reshape | solution.py:115
  161.4 17.1 %fusion.2 = f32[8,320,896]{2,1,0:T(8,128)} fusion(bf16[8,320,2048]{2,1,0:T(8,128)(2,1)} %reshape.121, bf16[1,2048,896]{2,1,0:T(8,128)(2,1)} %param.27), kind=kOutput, calls=%fused_computation.5 | convolution fusion | flops 9395240960 | bytes 23330816 | tf_op jit(solution)/shard_map/vmap()/dot_general | solution.py:117
  178.6 14.0 %multiply_convert_fusion = bf16[8,320,896]{2,1,0:T(8,128)(2,1)S(1)} fusion(f32[8,320,896]{2,1,0:T(8,128)} %fusion.2, bf16[8,320,2048]{2,1,0:T(8,128)(2,1)S(1)} %copy-done, bf16[1,2048,896]{2,1,0:T(8,128)(2,1)S(1)} %copy-done.7), kind=kOutput, calls=%fused_computation.2 | convolution fusion | flops 9409003520 | bytes 27918336 | tf_op jit(solution)/shard_map/vmap()/dot_general | solution.py:116
  192.6 4.7 %copy.63 = bf16[8,320,896]{2,0,1:T(8,128)(2,1)} copy(bf16[8,320,896]{2,1,0:T(8,128)(2,1)S(1)} %multiply_convert_fusion) | data formatting | bytes 9175040 | tf_op jit(solution)/shard_map/vmap()/convert_element_type | solution.py:118
  197.3 18.0 %convert_bitcast_fusion = bf16[16,8,20,2048]{3,2,0,1:T(8,128)(2,1)} fusion(bf16[8,16,20,896]{3,0,2,1:T(8,128)(2,1)} %bitcast.114, bf16[1,896,2048]{2,1,0:T(8,128)(2,1)S(1)} %copy-done.8), kind=kOutput, calls=%fused_computation.1 | convolution fusion | flops 9400483840 | bytes 18743296 | tf_op jit(solution)/shard_map/vmap()/dot_general | solution.py:119
  215.3 72.8 %reduce-scatter.2.cloned.1.call-done = bf16[16,1,20,2048]{3,2,0,1:T(8,128)(2,1)} async-done(((bf16[16,8,20,2048]{3,2,0,1:T(8,128)(2,1)}), bf16[16,1,20,2048]{3,2,0,1:T(8,128)(2,1)}) %reduce-scatter.2.cloned.1.call-update) | async-done | bytes 1310736 | tf_op jit(solution)/shard_map/reduce_scatter | solution.py:123
  288.2 6.9 %all-to-all-start.3 = ((bf16[16,20,2048]{2,1,0:T(8,128)(2,1)}), bf16[16,20,2048]{2,1,0:T(8,128)(2,1)S(1)}, u32[]{:S(2)}, u32[]{:S(2)}) async-start(bf16[16,20,2048]{2,1,0:T(8,128)(2,1)} %bitcast.115), calls=%async_computation.4 | async-start | bytes 3145728 | tf_op jit(solution)/shard_map/all_to_all | solution.py:125
  295.1 0.1 mul.548
  295.3 0.1 copy.65
  295.4 23.2 %all-to-all-done.3 = bf16[16,20,2048]{2,1,0:T(8,128)(2,1)S(1)} async-done(((bf16[16,20,2048]{2,1,0:T(8,128)(2,1)}), bf16[16,20,2048]{2,1,0:T(8,128)(2,1)S(1)}, u32[]{:S(2)}, u32[]{:S(2)}) %all-to-all-start.3) | async-done | bytes 1310752 | tf_op jit(solution)/shard_map/all_to_all | solution.py:125
  318.6 0.3 reshape.124
  318.9 2.3 gather_fusion
  321.3 2.4 reshape.125
  323.7 3.2 multiply_reduce_fusion
  326.9 0.2 multiply_reduce_fusion.1
  327.0 1.2 add_convert_fusion
  (41 shorter events, 0.4 us)
Async XLA Ops:
  7.7 7.5 %collective-permute-start = (bf16[30,128]{1,0:T(8,128)(2,1)S(1)}, bf16[30,128]{1,0:T(8,128)(2,1)S(1)}, u32[]{:S(2)}, u32[]{:S(2)}) collective-permute-start(bf16[30,128]{1,0:T(8,128)(2,1)S(1)} %slice.271), channel_id=1, source_target_pairs={{0,8},{8,16},{16,24},{24,32},{32,40},{40,48},{48,56},{56,64},{64,7... | collective-permute-start | bytes 23048 | tf_op jit(solution)/shard_map/ppermute | solution.py:13
  15.3 17.8 %copy-start.3 = (bf16[2048]{0:T(1024)(128)(2,1)S(1)}, bf16[2048]{0:T(1024)(128)(2,1)}, u32[]{:S(2)}) copy-start(bf16[2048]{0:T(1024)(128)(2,1)} %param.22) | copy-start | bytes 12292
  15.3 17.9 %copy-start.4 = (bf16[2048]{0:T(1024)(128)(2,1)S(1)}, bf16[2048]{0:T(1024)(128)(2,1)}, u32[]{:S(2)}) copy-start(bf16[2048]{0:T(1024)(128)(2,1)} %param.23) | copy-start | bytes 12292
  17.7 26.1 %copy-start.1 = (bf16[128,2048]{1,0:T(8,128)(2,1)S(1)}, bf16[128,2048]{1,0:T(8,128)(2,1)}, u32[]{:S(2)}) copy-start(bf16[128,2048]{1,0:T(8,128)(2,1)} %param.21) | copy-start | bytes 1572868
  18.4 10.1 %all-to-all-start = ((f32[8,1,2048]{2,1,0:T(1,128)}), f32[8,1,2048]{2,1,0:T(1,128)S(1)}, u32[]{:S(2)}, u32[]{:S(2)}) async-start(f32[8,1,2048]{2,1,0:T(1,128)} %broadcast_in_dim.2), calls=%async_computation | async-start | bytes 131072 | tf_op jit(solution)/shard_map/all_to_all | solution.py:18
  29.6 10.9 %all-to-all-start.1 = ((bf16[8,128,128]{2,1,0:T(8,128)(2,1)}), bf16[8,128,128]{2,1,0:T(8,128)(2,1)S(1)}, u32[]{:S(2)}, u32[]{:S(2)}) async-start(bf16[8,128,128]{2,1,0:T(8,128)(2,1)} %bitcast.31), calls=%async_computation.1 | async-start | bytes 524288 | tf_op jit(solution)/shard_map/all_to_all | solution.py:84
  33.0 98.0 %all-gather.3.cloned.1.call-start = ((), (), s32[]{:S(2)}) async-start(), calls=%async_computation.6 | async-start | bytes 11796480 | tf_op jit(solution)/shard_map/all_gather | solution.py:43
  76.8 211.4 %reduce-scatter.2.cloned.1.call-start = ((), (), s32[]{:S(2)}) async-start(), calls=%async_computation.5 | async-start | bytes 14155776 | tf_op jit(solution)/shard_map/reduce_scatter | solution.py:123
  161.4 17.1 %copy-start = (bf16[8,320,2048]{2,1,0:T(8,128)(2,1)S(1)}, bf16[8,320,2048]{2,1,0:T(8,128)(2,1)}, u32[]{:S(2)}) copy-start(bf16[8,320,2048]{2,1,0:T(8,128)(2,1)} %reshape.121) | copy-start | bytes 31457284
  161.4 17.1 %copy-start.7 = (bf16[1,2048,896]{2,1,0:T(8,128)(2,1)S(1)}, bf16[1,2048,896]{2,1,0:T(8,128)(2,1)}, u32[]{:S(2)}) copy-start(bf16[1,2048,896]{2,1,0:T(8,128)(2,1)} %param.26) | copy-start | bytes 11010052
  192.6 4.7 %copy-start.8 = (bf16[1,896,2048]{2,1,0:T(8,128)(2,1)S(1)}, bf16[1,896,2048]{2,1,0:T(8,128)(2,1)}, u32[]{:S(2)}) copy-start(bf16[1,896,2048]{2,1,0:T(8,128)(2,1)} %param.28) | copy-start | bytes 11010052
  215.3 79.9 %copy-start.6 = (f32[128,2]{0,1:T(2,128)S(1)}, f32[128,2]{0,1:T(2,128)}, u32[]{:S(2)}) copy-start(f32[128,2]{0,1:T(2,128)} %param.25) | copy-start | bytes 3076
  215.3 80.1 %copy-start.5 = (bf16[2048]{0:T(1024)(128)(2,1)S(1)}, bf16[2048]{0:T(1024)(128)(2,1)}, u32[]{:S(2)}) copy-start(bf16[2048]{0:T(1024)(128)(2,1)} %param.29) | copy-start | bytes 12292
  288.2 30.5 %all-to-all-start.3 = ((bf16[16,20,2048]{2,1,0:T(8,128)(2,1)}), bf16[16,20,2048]{2,1,0:T(8,128)(2,1)S(1)}, u32[]{:S(2)}, u32[]{:S(2)}) async-start(bf16[16,20,2048]{2,1,0:T(8,128)(2,1)} %bitcast.115), calls=%async_computation.4 | async-start | bytes 3145728 | tf_op jit(solution)/shard_map/all_to_all | solution.py:125
  321.3 5.8 %copy-start.2 = (bf16[128,2048]{1,0:T(8,128)(2,1)S(1)}, bf16[128,2048]{1,0:T(8,128)(2,1)}, u32[]{:S(2)}) copy-start(bf16[128,2048]{1,0:T(8,128)(2,1)} %param.21) | copy-start | bytes 1572868
Sparse Core Ops, SparseCore 0:
  76.9 54.0 all-gather.2
  215.4 72.6 reduce-scatter.1
where the time goes:
time: 339 us; the launch traced here: 335 us
  waiting for transfers between devices  163 us (48%)
  matrix products  52.8 us (16%)
  local copies, waits for them, and re-layouts  44.9 us (13%)
  blocking collectives  29.8 us (9%)
  starting transfers between devices  18.6 us (5%)
  between operations  13.7 us (4%)
  other arithmetic  12.7 us (4%)
    reduce_scatter x1, waiting for transfers between devices, per_device(): lax.psum_scatter(partials.astype(jnp.bfloat16), 'tp', scatter_dimension=1...  72.8 us
    all_gather x1, waiting for transfers between devices, work_in_pieces(): blocks = [lax.all_gather(piece, axis) for piece in pieces]  54 us
    all_to_all x1, blocking collectives, per_device(): lax.all_to_all(outgoing, 'sp', split_axis=0, concat_axis=0, tiled=True)  29.8 us
    all_to_all x1, waiting for transfers between devices, per_device(): lax.all_to_all(own_results, 'sp', split_axis=0, concat_axis=0, tiled=True)  23.2 us
    dot_general x1, matrix products, expert_terms(): jnp.dot(hidden, w_down, preferred_element_type=jnp.float32)  18 us
    dot_general x1, matrix products, expert_terms(): up_proj = jnp.dot(flat_rows, w_up, preferred_element_type=jnp.float32)  17.1 us
    reshape x1, local copies, waits for them, and re-layouts, expert_terms(): flat_rows = block_rows.reshape(-1, piece_dims[-1])  16.5 us
    dot_general x1, matrix products, expert_terms(): gate_proj = jnp.dot(flat_rows, w_gate, preferred_element_type=jnp.float32)  14 us
  transfers between devices with their start and end apart: 6, of which 5 were waited for; matrix products, arithmetic and copies ran while one was open for 1% of the time, Pallas kernels for 0%

commit v1 on v0

v1 whole, which is shorter than its diff:
```python
import functools

import jax
import jax.numpy as jnp
from jax import lax
from jax.experimental import pallas as pl
from jax.experimental.pallas import tpu as pltpu
from jax.sharding import PartitionSpec as P

D = 2048
D_A = 1024
HALF = D // 2
FFB = 896
CAP = 20
PAD = 24
TOK = 128
NG = 4
ROWS = 4 * CAP
PADROWS = 4 * PAD
MESH = pl.DeviceIdType.MESH
BF16 = jnp.bfloat16
F32 = jnp.float32

GROUPS = (
    ((0, 1), (0, 3), (1, 0), (3, 0)),
    ((0, 0), (0, 2), (2, 0), (2, 2)),
    ((2, 1), (2, 3), (1, 2), (3, 2)),
    ((1, 1), (1, 3), (3, 1), (3, 3)),
)
OFFS = tuple(o for g in GROUPS for o in g)
SELF = OFFS.index((0, 0))


def moe_kernel(
    normed_ref,
    stream_ref,
    disp_ref,
    comb_ref,
    gain_ref,
    wg_hbm,
    wu_hbm,
    wd_hbm,
    out_ref,
    wgu,
    wd,
    outg,
    arecv,
    xbuf,
    hbuf,
    pbuf,
    precv,
    r1,
    r2,
    ret_s,
    ret_r,
    wsem,
    a_s,
    a_r,
    g_s,
    g_r,
    s_s,
    s_r,
    t_s,
    t_r,
):
    sp = lax.axis_index("sp")
    tp = lax.axis_index("tp")
    z, x = lax.div(sp, 4), lax.rem(sp, 4)
    y, c = lax.div(tp, 2), lax.rem(tp, 2)

    def sp_at(dz, dx):
        return lax.rem(z + dz, 4) * 4 + lax.rem(x + dx, 4)

    up = lax.rem(y + 1, 4) * 2 + c
    down = lax.rem(y + 3, 4) * 2 + c
    mate = y * 2 + 1 - c

    wcopies = []
    for j in range(7):
        cols = pl.ds(128 * j, 128)
        for h, w in enumerate((wg_hbm, wu_hbm)):
            wcopies.append(
                pltpu.make_async_copy(
                    w.at[0, :, cols], wgu.at[j, :, pl.ds(128 * h, 128)], wsem.at[2 * j + h]
                )
            )
    wcopies.append(pltpu.make_async_copy(wd_hbm.at[0], wd, wsem.at[14]))
    for cp in wcopies:
        cp.start()

    barrier = pltpu.get_barrier_semaphore()
    for o in OFFS:
        if o != (0, 0):
            pl.semaphore_signal(
                barrier, inc=1, device_id={"sp": sp_at(*o), "tp": tp}, device_id_type=MESH
            )
    for t in (up, down, mate):
        pl.semaphore_signal(barrier, inc=1, device_id={"sp": sp, "tp": t}, device_id_type=MESH)
    pl.semaphore_wait(barrier, 18)

    def remote(src, dst, ssem, rsem, spi, tpi):
        return pltpu.make_async_remote_copy(
            src_ref=src,
            dst_ref=dst,
            send_sem=ssem,
            recv_sem=rsem,
            device_id={"sp": spi, "tp": tpi},
            device_id_type=MESH,
        )

    sends = []

    acopies = {}
    for i in range(NG):
        rows = jnp.dot(
            disp_ref[PADROWS * i : PADROWS * (i + 1), :],
            normed_ref[...],
            preferred_element_type=F32,
        )
        outg[4 * i : 4 * i + 4] = rows.astype(BF16).reshape(4, PAD, D)
        for j in range(4 * i, 4 * i + 4):
            if j != SELF:
                acopies[j] = remote(
                    outg.at[j], arecv.at[j], a_s.at[j], a_r.at[j], sp_at(*OFFS[j]), tp
                )
                acopies[j].start()
                sends.append(acopies[j])

    r_i = lax.broadcasted_iota(jnp.int32, (ROWS, PADROWS), 0)
    c_i = lax.broadcasted_iota(jnp.int32, (ROWS, PADROWS), 1)
    q_i = sum((r_i >= CAP * k).astype(jnp.int32) for k in (1, 2, 3))
    compact = (c_i == r_i + (PAD - CAP) * q_i).astype(F32).astype(BF16)
    r_e = lax.broadcasted_iota(jnp.int32, (PADROWS, ROWS), 0)
    c_e = lax.broadcasted_iota(jnp.int32, (PADROWS, ROWS), 1)
    q_e = sum((c_e >= CAP * k).astype(jnp.int32) for k in (1, 2, 3))
    expand = (r_e == c_e + (PAD - CAP) * q_e).astype(F32).astype(BF16)

    ag = [dict() for _ in range(NG)]

    def ag_copy(i, n, src, dst, tpi):
        cp = remote(src, dst, g_s.at[i, n], g_r.at[i, n], sp, tpi)
        cp.start()
        ag[i][n] = cp
        sends.append(cp)

    def gather1(i):
        blocks = []
        for j in range(4 * i, 4 * i + 4):
            if j == SELF:
                blocks.append(outg[j])
            else:
                acopies[j].wait_recv()
                blocks.append(arecv[j])
        own = jnp.dot(compact, jnp.concatenate(blocks, axis=0), preferred_element_type=F32)
        xbuf[i, 0, 0] = own.astype(BF16)
        src = xbuf.at[i, 0, 0]
        ag_copy(i, 0, src, xbuf.at[i, 0, 3], up)
        ag_copy(i, 1, src, xbuf.at[i, 0, 1], down)
        ag_copy(i, 2, src, xbuf.at[i, 1, 0], mate)

    lo, hi = pl.ds(0, HALF), pl.ds(HALF, HALF)

    def gather2(i):
        ag[i][0].wait_recv()
        ag_copy(i, 3, xbuf.at[i, 0, 3, :, lo], xbuf.at[i, 0, 2, :, lo], up)
        ag_copy(i, 6, xbuf.at[i, 0, 3], xbuf.at[i, 1, 3], mate)
        ag[i][1].wait_recv()
        ag_copy(i, 4, xbuf.at[i, 0, 1, :, hi], xbuf.at[i, 0, 2, :, hi], down)
        ag_copy(i, 5, xbuf.at[i, 0, 1], xbuf.at[i, 1, 1], mate)

    def gather3(i):
        ag[i][3].wait_recv()
        ag[i][4].wait_recv()
        ag_copy(i, 7, xbuf.at[i, 0, 2], xbuf.at[i, 1, 2], mate)
        for n in (2, 5, 6, 7):
            ag[i][n].wait_recv()

    rs = [dict() for _ in range(NG)]

    def rs_copy(i, n, src, dst, tpi):
        cp = remote(src, dst, s_s.at[i, n], s_r.at[i, n], sp, tpi)
        cp.start()
        rs[i][n] = cp
        sends.append(cp)

    def experts(i):
        if i == 0:
            for cp in wcopies[:14]:
                cp.wait()

        @pl.loop(0, 7)
        def _(j):
            gu = jnp.dot(xbuf[i].reshape(8 * ROWS, D), wgu[j], preferred_element_type=F32)
            g, u = gu[:, :128], gu[:, 128:]
            h = g * (1.0 / (1.0 + jnp.exp(-g))) * u
            hbuf[:, pl.ds(pl.multiple_of(j * 128, 128), 128)] = h.astype(BF16)

        if i == 0:
            wcopies[14].wait()
        for half in (1, 0):

            @pl.loop(0, 8)
            def _(n):
                cols = pl.ds(pl.multiple_of(n * 256, 256), 256)
                p = jnp.dot(
                    hbuf[4 * ROWS * half : 4 * ROWS * (half + 1), :],
                    wd[:, cols],
                    preferred_element_type=F32,
                )
                pbuf[i, half, :, :, cols] = p.astype(BF16).reshape(4, ROWS, 256)

            if half == 1:
                rs_copy(i, 0, pbuf.at[i, 1], precv.at[i], mate)

    def both(i, k, cols):
        return pbuf[i, 0, k, :, cols].astype(F32) + precv[i, k, :, cols].astype(F32)

    def scatter1(i):
        rs[i][0].wait_recv()
        pbuf[i, 0, 2] = both(i, 2, slice(None)).astype(BF16)
        rs_copy(i, 1, pbuf.at[i, 0, 2, :, lo], r1.at[i, 0], up)
        rs_copy(i, 2, pbuf.at[i, 0, 2, :, hi], r1.at[i, 1], down)
        pbuf[i, 0, 1, :, HALF:] = both(i, 1, slice(HALF, D)).astype(BF16)
        rs_copy(i, 3, pbuf.at[i, 0, 1, :, hi], r2.at[i, 0, :, hi], up)
        pbuf[i, 0, 3, :, :HALF] = both(i, 3, slice(0, HALF)).astype(BF16)
        rs_copy(i, 4, pbuf.at[i, 0, 3, :, lo], r2.at[i, 1, :, lo], down)

    def scatter2(i):
        rs[i][1].wait_recv()
        pbuf[i, 0, 1, :, :HALF] = (both(i, 1, slice(0, HALF)) + r1[i, 0].astype(F32)).astype(BF16)
        rs_copy(i, 5, pbuf.at[i, 0, 1, :, lo], r2.at[i, 0, :, lo], up)
        rs[i][2].wait_recv()
        pbuf[i, 0, 3, :, HALF:] = (both(i, 3, slice(HALF, D)) + r1[i, 1].astype(F32)).astype(BF16)
        rs_copy(i, 6, pbuf.at[i, 0, 3, :, hi], r2.at[i, 1, :, hi], down)

    tcopies = {}

    def give_back(i):
        for n in (3, 4, 5, 6):
            rs[i][n].wait_recv()
        total = both(i, 0, slice(None)) + r2[i, 0].astype(F32) + r2[i, 1].astype(F32)
        padded = jnp.dot(expand, total.astype(BF16), preferred_element_type=F32)
        padded = padded.astype(BF16).reshape(4, PAD, D)
        for q in range(4):
            j = 4 * i + q
            dz, dx = OFFS[j]
            if j == SELF:
                ret_r[j] = padded[q]
            else:
                ret_s[j] = padded[q]
                tcopies[j] = remote(
                    ret_s.at[j], ret_r.at[j], t_s.at[j], t_r.at[j], sp_at(4 - dz, 4 - dx), tp
                )
                tcopies[j].start()
                sends.append(tcopies[j])

    gather1(0)
    gather1(1)
    gather2(0)
    gather1(2)
    gather2(1)
    gather3(0)
    experts(0)
    scatter1(0)
    gather1(3)
    gather2(2)
    scatter2(0)
    gather3(1)
    experts(1)
    scatter1(1)
    gather2(3)
    scatter2(1)
    gather3(2)
    experts(2)
    scatter1(2)
    give_back(0)
    scatter2(2)
    gather3(3)
    experts(3)
    scatter1(3)
    give_back(1)
    scatter2(3)
    give_back(2)
    give_back(3)
    for j in range(16):
        if j != SELF:
            tcopies[j].wait_recv()
    ret = ret_r[...].reshape(16 * PAD, D)
    mix = jnp.dot(comb_ref[0], ret, preferred_element_type=F32)
    mix = mix + jnp.dot(comb_ref[1], ret, preferred_element_type=F32)
    scale = lax.rsqrt(jnp.mean(mix * mix, axis=1, keepdims=True) + 1e-06)
    out_ref[...] = (stream_ref[...] + mix * scale * gain_ref[...].astype(F32)).astype(BF16)
    for cp in sends:
        cp.wait_send()


def moe(normed, stream, disp, comb, gain, wg, wu, wd):
    vmem = pl.BlockSpec(memory_space=pltpu.VMEM)
    hbm = pl.BlockSpec(memory_space=pl.ANY)
    dma = pltpu.SemaphoreType.DMA
    return pl.pallas_call(
        moe_kernel,
        out_shape=jax.ShapeDtypeStruct((TOK, D), BF16),
        in_specs=[vmem] * 5 + [hbm] * 3,
        out_specs=vmem,
        scratch_shapes=[
            pltpu.VMEM((7, D, 256), BF16),
            pltpu.VMEM((FFB, D), BF16),
            pltpu.VMEM((16, PAD, D), BF16),
            pltpu.VMEM((16, PAD, D), BF16),
            pltpu.VMEM((NG, 2, 4, ROWS, D), BF16),
            pltpu.VMEM((8 * ROWS, FFB), BF16),
            pltpu.VMEM((NG, 2, 4, ROWS, D), BF16),
            pltpu.VMEM((NG, 4, ROWS, D), BF16),
            pltpu.VMEM((NG, 2, ROWS, HALF), BF16),
            pltpu.VMEM((NG, 2, ROWS, D), BF16),
            pltpu.VMEM((16, PAD, D), BF16),
            pltpu.VMEM((16, PAD, D), BF16),
            dma((15,)),
            dma((16,)),
            dma((16,)),
            dma((NG, 8)),
            dma((NG, 8)),
            dma((NG, 7)),
            dma((NG, 7)),
            dma((16,)),
            dma((16,)),
        ],
        compiler_params=pltpu.CompilerParams(
            collective_id=0, has_side_effects=True, vmem_limit_bytes=62 * 1024 * 1024
        ),
        name="moe",
    )(normed, stream, disp, comb, gain, wg, wu, wd)


def passed_along(value, axis, steps):
    count = lax.axis_size(axis)
    leading, last = (max(0, -steps), min(count, count - steps))
    return lax.ppermute(value, axis, [(source, source + steps) for source in range(leading, last)])


def copy_for_each(value, axis):
    copies = jnp.broadcast_to(value, (lax.axis_size(axis), *value.shape))
    return lax.all_to_all(copies, axis, split_axis=0, concat_axis=0, tiled=True)


def over_copies(value, axis):
    return copy_for_each(value, axis).sum(axis=0)


def together(arrays, axis):
    ends = [0]
    for a in arrays:
        ends.append(ends[-1] + a.size)
    subtotal = over_copies(jnp.concatenate([a.ravel() for a in arrays]), axis)
    return tuple((subtotal[b:e].reshape(a.shape) for a, b, e in zip(arrays, ends, ends[1:])))


def route_tables(routes, route_weights):
    sp = lax.axis_index("sp")
    z, x = sp // 4, sp % 4
    flat = routes.reshape(-1)
    experts = jnp.arange(16, dtype=jnp.int32)
    matches = (flat[:, None] == experts[None, :]).astype(jnp.int32)
    before = jnp.cumsum(matches, axis=0) - matches
    slot = jnp.sum(before * matches, axis=1)
    rel = ((flat // 4 - z) % 4) * 4 + (flat % 4 - x) % 4
    place = jnp.zeros_like(rel)
    for j, (dz, dx) in enumerate(OFFS):
        place = place + jnp.where(rel == dz * 4 + dx, j, 0)
    target = (place * PAD + slot).reshape(TOK, 2)
    slots = jnp.arange(16 * PAD, dtype=jnp.int32)
    disp = jnp.any(target.T[:, None, :] == slots[None, :, None], axis=0).astype(BF16)
    hits = target[:, :, None] == slots[None, None, :]
    comb = jnp.sum(jnp.where(hits, route_weights[:, :, None], 0.0), axis=1)
    high = comb.astype(BF16)
    low = (comb - high.astype(F32)).astype(BF16)
    return disp, jnp.stack([high, low])


def per_device(
    a_lin,
    a_gate,
    conv_weight,
    ln_gain,
    ln_bias,
    proj_weight,
    residual,
    mix_gain,
    ffn_gain,
    routes,
    route_weights,
    gate_weight,
    up_weight,
    down_weight,
    out_gain,
):
    kernel_len = conv_weight.shape[0]
    gated = (a_lin.astype(jnp.float32) * jax.nn.sigmoid(a_gate.astype(jnp.float32))).astype(
        jnp.bfloat16
    )
    row_count = gated.shape[0]
    edge_rows = passed_along(gated[row_count - (kernel_len - 1) :], "sp", 1)
    padded = jnp.concatenate([edge_rows, gated], 0).astype(jnp.float32)
    filter_taps = conv_weight.astype(jnp.float32)
    conv_out = filter_taps[0] * padded[0:row_count]
    for offset in range(1, kernel_len):
        conv_out = conv_out + filter_taps[offset] * padded[offset : offset + row_count]
    row_total, squares = together(
        (jnp.sum(conv_out, axis=1), jnp.sum(conv_out * conv_out, axis=1)), "tp"
    )
    row_mean = row_total / D_A
    row_var = squares / D_A - row_mean * row_mean
    scaled = (conv_out - row_mean[:, None]) * lax.rsqrt(row_var[:, None] + 1e-05)
    scaled = scaled * ln_gain.astype(jnp.float32) + ln_bias.astype(jnp.float32)
    activated = jax.nn.silu(scaled).astype(jnp.bfloat16)
    token_acts = lax.all_to_all(activated, "tp", split_axis=0, concat_axis=1, tiled=True)
    branch = jnp.dot(token_acts, proj_weight, preferred_element_type=jnp.float32)
    branch_f = lax.optimization_barrier(branch.astype(jnp.bfloat16)).astype(jnp.float32)
    branch_scale = lax.rsqrt(jnp.mean(branch_f * branch_f, axis=1, keepdims=True) + 1e-06)
    stream = residual.astype(jnp.float32) + branch_f * branch_scale * mix_gain.astype(jnp.float32)
    stream_scale = lax.rsqrt(jnp.mean(stream * stream, axis=1, keepdims=True) + 1e-06)
    normed = (stream * stream_scale * ffn_gain.astype(jnp.float32)).astype(jnp.bfloat16)
    disp, comb = route_tables(routes, route_weights)
    return moe(
        normed, stream, disp, comb, out_gain.reshape(1, D), gate_weight, up_weight, down_weight
    )


def solution(mesh):
    return jax.shard_map(
        per_device,
        mesh=mesh,
        in_specs=(
            P("sp", "tp"),
            P("sp", "tp"),
            P(None, "tp"),
            P("tp"),
            P("tp"),
            P(),
            P(("sp", "tp"), None),
            P(),
            P(),
            P(("sp", "tp"), None),
            P(("sp", "tp"), None),
            P("sp", None, "tp"),
            P("sp", None, "tp"),
            P("sp", "tp", None),
            P(),
        ),
        out_specs=P(("sp", "tp"), None),
        check_vma=False,
    )
```

time: 339 us -> 179 us (0.53); the launches traced: 335 us -> 179 us
  waiting for transfers between devices: 163 us -> 10.7 us
  Pallas kernels: 0 us -> 137 us
  matrix products: 52.8 us -> 2.94 us
  local copies, waits for them, and re-layouts: 44.9 us -> 5.1 us
  blocking collectives: 29.8 us -> 0 us
  between operations: 13.7 us -> 0.31 us
  starting transfers between devices: 18.6 us -> 11.6 us
    pallas_call x0 -> x1, Pallas kernels: none -> 137 us  [moe(): pl.pallas_call(moe_kernel, out_shape=jax.ShapeDtypeStruct((TOK, D), BF16)...]
    reduce_scatter x1 -> x0, waiting for transfers between devices: 72.8 us -> none  [per_device(): lax.psum_scatter(partials.astype(jnp.bfloat16), 'tp', scatter_dimension=1...]
    all_gather x1 -> x0, waiting for transfers between devices: 54 us -> none  [work_in_pieces(): blocks = [lax.all_gather(piece, axis) for piece in pieces]]
    dot_general x4 -> x0, matrix products: 49.8 us -> none  [the longest x1 18 us: expert_terms(): jnp.dot(hidden, w_down, preferred_element_type=jnp.float32)]
    all_to_all x1 -> x0, blocking collectives: 29.8 us -> none  [per_device(): lax.all_to_all(outgoing, 'sp', split_axis=0, concat_axis=0, tiled=True)]
    all_to_all x1 -> x0, waiting for transfers between devices: 23.2 us -> none  [per_device(): lax.all_to_all(own_results, 'sp', split_axis=0, concat_axis=0, tiled=True)]
    reshape x3 -> x1, local copies, waits for them, and re-layouts: 17.1 us -> 0.6 us  [per_device(): out_gain.reshape(1, D)]
    all_gather x1 -> x0, local copies, waits for them, and re-layouts: 14 us -> none  [work_in_pieces(): blocks = [lax.all_gather(piece, axis) for piece in pieces]]
  transfers between devices with their start and end apart: 6 -> 3, of which waited for: 5 -> 2; matrix products, arithmetic and copies ran while one was open for 1% -> 4% of each run, Pallas kernels for 0% -> 0%
where the time goes in v1:
time: 179 us
  Pallas kernels  137 us (77%)
  starting transfers between devices  11.6 us (6%)
  other arithmetic  11.1 us (6%)
  waiting for transfers between devices  10.7 us (6%)
  local copies, waits for them, and re-layouts  5.1 us (3%)
  matrix products  2.94 us (2%)
    pallas_call x1, Pallas kernels, moe(): pl.pallas_call(moe_kernel, out_shape=jax.ShapeDtypeStruct((TOK, D), BF16)...  137 us
    all_to_all x1, waiting for transfers between devices, per_device(): lax.all_to_all(activated, 'tp', split_axis=0, concat_axis=1, tiled=True)  5.84 us
    all_to_all x1, waiting for transfers between devices, copy_for_each(): return lax.all_to_all(copies, axis, split_axis=0, concat_axis=0, tiled=True)  4.83 us
    all_to_all x1, starting transfers between devices, copy_for_each(): return lax.all_to_all(copies, axis, split_axis=0, concat_axis=0, tiled=True)  4.47 us
    all_to_all x1, starting transfers between devices, per_device(): lax.all_to_all(activated, 'tp', split_axis=0, concat_axis=1, tiled=True)  3.59 us
  transfers between devices with their start and end apart: 3, of which 2 were waited for; matrix products, arithmetic and copies ran while one was open for 4% of the time, Pallas kernels for 0%

profile of v1, /device:TPU:0, one launch (start us, length us, event | category | flops | bytes accessed | tf_op | source)
XLA Modules:
  0.0 178.9 jit_solution(9451627340053858907)
XLA Ops:
  0.0 1.2 multiply_convert_fusion.2
  1.2 3.5 %collective-permute-start = (bf16[30,128]{1,0:T(8,128)(2,1)S(1)}, bf16[30,128]{1,0:T(8,128)(2,1)S(1)}, u32[]{:S(2)}, u32[]{:S(2)}) collective-permute-start(bf16[30,128]{1,0:T(8,128)(2,1)S(1)} %slice.269), channel_id=1, source_target_pairs={{0,8},{8,16},{16,24},{24,32},{32,40},{40,48},{48,56},{56,64},{64,7... | collective-permute-start | bytes 23048 | tf_op jit(solution)/shard_map/ppermute | solution.py:339
  4.7 0.7 convert_element_type.87
  5.5 0.7 broadcast_compare_fusion
  6.1 0.8 copy.58
  6.9 0.1 eq.199
  7.1 0.1 eq.203
  7.2 0.1 copy.63
  7.4 0.6 reduce-window.6
  8.0 0.2 slice_reduce_fusion
  8.2 0.1 fusion.44
  8.3 0.1 reduce_sum.73
  8.4 0.2 multiply_add_fusion
  8.7 0.1 copy.69
  8.7 0.8 select_reduce_fusion
  9.6 0.0 collective-permute-done
  9.6 0.1 maximum_convert_fusion
  9.7 0.0 copy-start.5
  9.7 0.0 copy-start.6
  9.7 0.0 copy-start.2
  9.7 0.0 copy-start.3
  9.7 0.0 copy-start.4
  9.7 2.4 %fusion.49 = (f32[1024]{0:T(1024)S(1)}, f32[1024]{0:T(1024)S(1)}, f32[1024,128]{1,0:T(8,128)S(1)}) fusion(f32[1054,128]{1,0:T(8,128)S(1)} %maximum_convert_fusion, f32[128]{0:T(128)S(1)} %get-tuple-element.13, f32[128]{0:T(128)S(1)} %get-tuple-element.14, f32[128]{0:T(128)S(1)} %get-tuple-element.15, f32[128]{0:T(128)S(1)} %get-tuple-element.16, ...), kind=kLoop, calls=%fused_computation.150 | loop fusion | flops 8386560 | bytes 16801280 | tf_op jit(solution)/shard_map/reduce_sum | solution.py:410
  12.1 0.7 broadcast_in_dim.70
  12.8 4.5 %all-to-all-start = ((f32[8,1,2048]{2,1,0:T(1,128)}), f32[8,1,2048]{2,1,0:T(1,128)S(1)}, u32[]{:S(2)}, u32[]{:S(2)}) async-start(f32[8,1,2048]{2,1,0:T(1,128)} %broadcast_in_dim.70), calls=%async_computation | async-start | bytes 131072 | tf_op jit(solution)/shard_map/all_to_all | solution.py:344
  17.3 0.0 copy-done.5
  17.3 0.0 copy-done.6
  17.3 0.0 copy-done.2
  17.4 0.0 copy-done.3
  17.4 0.0 copy-done.4
  17.4 0.6 reshape.179.gain_ref
  18.0 0.1 copy.68
  18.0 4.8 %all-to-all-done = f32[8,1,2048]{2,1,0:T(1,128)S(1)} async-done(((f32[8,1,2048]{2,1,0:T(1,128)}), f32[8,1,2048]{2,1,0:T(1,128)S(1)}, u32[]{:S(2)}, u32[]{:S(2)}) %all-to-all-start) | async-done | bytes 65568 | tf_op jit(solution)/shard_map/all_to_all | solution.py:344
  22.9 0.1 reduce_sum.69
  23.0 1.1 multiply_convert_fusion.1
  24.0 3.6 %all-to-all-start.1 = ((bf16[8,128,128]{2,1,0:T(8,128)(2,1)}), bf16[8,128,128]{2,1,0:T(8,128)(2,1)S(1)}, u32[]{:S(2)}, u32[]{:S(2)}) async-start(bf16[8,128,128]{2,1,0:T(8,128)(2,1)} %bitcast.31), calls=%async_computation.1 | async-start | bytes 524288 | tf_op jit(solution)/shard_map/all_to_all | solution.py:417
  27.7 0.7 convert_element_type.102.disp_ref
  28.3 0.7 pad_maximum_fusion.comb_ref
  29.0 5.8 %all-to-all-done.1 = bf16[8,128,128]{2,1,0:T(8,128)(2,1)S(1)} async-done(((bf16[8,128,128]{2,1,0:T(8,128)(2,1)}), bf16[8,128,128]{2,1,0:T(8,128)(2,1)S(1)}, u32[]{:S(2)}, u32[]{:S(2)}) %all-to-all-start.1) | async-done | bytes 262176 | tf_op jit(solution)/shard_map/all_to_all | solution.py:417
  34.9 0.2 copy.57
  35.1 2.9 %convolution_convert_fusion = bf16[128,2048]{1,0:T(8,128)(2,1)S(1)} fusion(bf16[128,1024]{0,1:T(8,128)(2,1)S(1)} %bitcast.93, bf16[1024,2048]{1,0:T(8,128)(2,1)} %param.20), kind=kOutput, calls=%fused_computation | convolution fusion | flops 537133056 | bytes 4980736 | tf_op jit(solution)/shard_map/dot_general | solution.py:418
  38.0 0.2 fusion
  38.2 0.0 copy-done.1
  38.2 0.4 multiply_reduce_fusion
  38.6 1.1 multiply_convert_fusion.normed_ref
  39.7 0.1 copy-done
  39.8 137.3 %moe.1 = bf16[128,2048]{1,0:T(8,128)(2,1)} custom-call(bf16[128,2048]{1,0:T(8,128)(2,1)} %multiply_convert_fusion.normed_ref, f32[128,2048]{1,0:T(8,128)} %copy-done, bf16[384,128]{1,0:T(8,128)(2,1)} %convert_element_type.102.disp_ref, bf16[2,128,384]{2,1,0:T(8,128)(2,1)} %pad_maximum_fusion.comb_ref, bf16[1,2048]{1,0:T(2,128)(2,1)} %reshape.179.gain_ref, ...), custom_call_target="tpu_custom_call" | custom-call | tf_op jit(solution)/shard_map/moe/pallas_call | solution.py:301
  177.0 1.9 %copy.82 = bf16[128,2048]{1,0:T(8,128)(2,1)} copy(bf16[128,2048]{1,0:T(8,128)(2,1)} %moe.1) | data formatting | bytes 1048576
  (18 shorter events, 0.2 us)
Async XLA Ops:
  1.2 8.4 %collective-permute-start = (bf16[30,128]{1,0:T(8,128)(2,1)S(1)}, bf16[30,128]{1,0:T(8,128)(2,1)S(1)}, u32[]{:S(2)}, u32[]{:S(2)}) collective-permute-start(bf16[30,128]{1,0:T(8,128)(2,1)S(1)} %slice.269), channel_id=1, source_target_pairs={{0,8},{8,16},{16,24},{24,32},{32,40},{40,48},{48,56},{56,64},{64,7... | collective-permute-start | bytes 23048 | tf_op jit(solution)/shard_map/ppermute | solution.py:339
  9.7 7.6 %copy-start.5 = (bf16[128]{0:T(256)(128)(2,1)S(1)}, bf16[128]{0:T(256)(128)(2,1)}, u32[]{:S(2)}) copy-start(bf16[128]{0:T(256)(128)(2,1)} %param.18) | copy-start | bytes 772
  9.7 7.6 %copy-start.6 = (bf16[128]{0:T(256)(128)(2,1)S(1)}, bf16[128]{0:T(256)(128)(2,1)}, u32[]{:S(2)}) copy-start(bf16[128]{0:T(256)(128)(2,1)} %param.19) | copy-start | bytes 772
  9.7 7.7 %copy-start.2 = (bf16[2048]{0:T(1024)(128)(2,1)S(1)}, bf16[2048]{0:T(1024)(128)(2,1)}, u32[]{:S(2)}) copy-start(bf16[2048]{0:T(1024)(128)(2,1)} %param.22) | copy-start | bytes 12292
  9.7 7.7 %copy-start.3 = (bf16[2048]{0:T(1024)(128)(2,1)S(1)}, bf16[2048]{0:T(1024)(128)(2,1)}, u32[]{:S(2)}) copy-start(bf16[2048]{0:T(1024)(128)(2,1)} %param.23) | copy-start | bytes 12292
  9.7 7.7 %copy-start.4 = (bf16[2048]{0:T(1024)(128)(2,1)S(1)}, bf16[2048]{0:T(1024)(128)(2,1)}, u32[]{:S(2)}) copy-start(bf16[2048]{0:T(1024)(128)(2,1)} %param.29) | copy-start | bytes 12292
  12.8 10.1 %all-to-all-start = ((f32[8,1,2048]{2,1,0:T(1,128)}), f32[8,1,2048]{2,1,0:T(1,128)S(1)}, u32[]{:S(2)}, u32[]{:S(2)}) async-start(f32[8,1,2048]{2,1,0:T(1,128)} %broadcast_in_dim.70), calls=%async_computation | async-start | bytes 131072 | tf_op jit(solution)/shard_map/all_to_all | solution.py:344
  17.3 20.9 %copy-start.1 = (bf16[128,2048]{1,0:T(8,128)(2,1)S(1)}, bf16[128,2048]{1,0:T(8,128)(2,1)}, u32[]{:S(2)}) copy-start(bf16[128,2048]{1,0:T(8,128)(2,1)} %param.21) | copy-start | bytes 1572868
  24.0 10.9 %all-to-all-start.1 = ((bf16[8,128,128]{2,1,0:T(8,128)(2,1)}), bf16[8,128,128]{2,1,0:T(8,128)(2,1)S(1)}, u32[]{:S(2)}, u32[]{:S(2)}) async-start(bf16[8,128,128]{2,1,0:T(8,128)(2,1)} %bitcast.31), calls=%async_computation.1 | async-start | bytes 524288 | tf_op jit(solution)/shard_map/all_to_all | solution.py:417
  38.6 1.2 copy-start

commit v2 on v1

--- a/solution.py
+++ b/solution.py
@@ -1,5 +1,3 @@
-import functools
-
 import jax
 import jax.numpy as jnp
 from jax import lax
@@ -17,6 +15,7 @@
 NG = 4
 ROWS = 4 * CAP
 PADROWS = 4 * PAD
+EDGE = 32
 MESH = pl.DeviceIdType.MESH
 BF16 = jnp.bfloat16
 F32 = jnp.float32
@@ -31,16 +30,34 @@
 SELF = OFFS.index((0, 0))
 
 
-def moe_kernel(
-    normed_ref,
-    stream_ref,
-    disp_ref,
-    comb_ref,
-    gain_ref,
+def layer_kernel(
+    lin_hbm,
+    gate_hbm,
+    taps_ref,
+    proj_hbm,
+    resid_hbm,
+    gains_ref,
+    routes_ref,
+    rweights_ref,
     wg_hbm,
     wu_hbm,
     wd_hbm,
     out_ref,
+    lin,
+    gatein,
+    resid,
+    proj,
+    gsrc,
+    taps,
+    gbuf,
+    padf,
+    conv,
+    act,
+    branch,
+    stream_ref,
+    normed_ref,
+    comb_ref,
+    disp_ref,
     wgu,
     wd,
     outg,
@@ -53,7 +70,10 @@
     r2,
     ret_s,
     ret_r,
+    isem,
     wsem,
+    c_s,
+    c_r,
     a_s,
     a_r,
     g_s,
@@ -75,6 +95,15 @@
     down = lax.rem(y + 3, 4) * 2 + c
     mate = y * 2 + 1 - c
 
+    icopies = [
+        pltpu.make_async_copy(src, dst, isem.at[n])
+        for n, (src, dst) in enumerate(
+            ((lin_hbm, lin), (gate_hbm, gatein), (resid_hbm, resid), (proj_hbm, proj))
+        )
+    ]
+    for cp in icopies:
+        cp.start()
+
     wcopies = []
     for j in range(7):
         cols = pl.ds(128 * j, 128)
@@ -89,14 +118,30 @@
         cp.start()
 
     barrier = pltpu.get_barrier_semaphore()
+
+    def greet(spi, tpi):
+        pl.semaphore_signal(
+            barrier, inc=1, device_id={"sp": spi, "tp": tpi}, device_id_type=MESH
+        )
+
+    for r in range(1, 8):
+        greet(sp, lax.rem(tp + r, 8))
     for o in OFFS:
         if o != (0, 0):
-            pl.semaphore_signal(
-                barrier, inc=1, device_id={"sp": sp_at(*o), "tp": tp}, device_id_type=MESH
-            )
-    for t in (up, down, mate):
-        pl.semaphore_signal(barrier, inc=1, device_id={"sp": sp, "tp": t}, device_id_type=MESH)
-    pl.semaphore_wait(barrier, 18)
+            greet(sp_at(*o), tp)
+
+    @pl.when(tp == 0)
+    def _():
+        for t in range(1, 8):
+            greet(lax.rem(sp + 15, 16), t)
+
+    icopies[0].wait()
+    icopies[1].wait()
+    for n in range(4):
+        rows = pl.ds(256 * n, 256)
+        g = gatein[rows, :].astype(F32)
+        gsrc[rows, :] = (lin[rows, :].astype(F32) * (1.0 / (1.0 + jnp.exp(-g)))).astype(BF16)
+    pl.semaphore_wait(barrier, 22 + jnp.minimum(tp, 1))
 
     def remote(src, dst, ssem, rsem, spi, tpi):
         return pltpu.make_async_remote_copy(
@@ -109,6 +154,134 @@
         )
 
     sends = []
+    ccopies = []
+
+    def exchange(n, src, dst, spi, tpi):
+        cp = remote(src, dst, c_s.at[n], c_r.at[n], spi, tpi)
+        cp.start()
+        ccopies.append(cp)
+        sends.append(cp)
+
+    def edge_of(t):
+        return pl.ds(pl.multiple_of(lax.rem(t + 7, 8) * TOK + TOK - EDGE, EDGE), EDGE)
+
+    def body_of(t):
+        return pl.ds(pl.multiple_of(t * TOK, TOK), TOK)
+
+    for r in range(1, 8):
+        t = lax.rem(tp + r, 8)
+        exchange(r - 1, gsrc.at[body_of(t)], gbuf.at[tp, pl.ds(EDGE, TOK)], sp, t)
+        first = lax.div(8 - t, 8)
+        exchange(
+            6 + r, gsrc.at[edge_of(t)], gbuf.at[tp, pl.ds(0, EDGE)], lax.rem(sp + first, 16), t
+        )
+    for r in range(1, 8):
+        exchange(13 + r, taps_ref, taps.at[tp], sp, lax.rem(tp + r, 8))
+    own_edge = remote(
+        gsrc.at[edge_of(0)],
+        gbuf.at[tp, pl.ds(0, EDGE)],
+        c_s.at[21],
+        c_r.at[21],
+        lax.rem(sp + 1, 16),
+        tp,
+    )
+
+    @pl.when(tp == 0)
+    def _():
+        own_edge.start()
+
+    @pl.when(tp > 0)
+    def _():
+        gbuf[tp, 0:EDGE] = gsrc[edge_of(tp), :]
+
+    gbuf[tp, EDGE:] = gsrc[body_of(tp), :]
+    taps[tp] = taps_ref[...]
+
+    lane = lax.broadcasted_iota(jnp.int32, (1, TOK), 1)
+    code = lax.broadcasted_iota(jnp.int32, (16, TOK), 0)
+    places, counts = [], jnp.zeros((16, TOK), F32)
+    for k in range(2):
+        e = routes_ref[k : k + 1, :]
+        ez, ex = lax.shift_right_logical(e, 2), jnp.bitwise_and(e, 3)
+        rel = jnp.bitwise_and(ez - z + 4, 3) * 4 + jnp.bitwise_and(ex - x + 4, 3)
+        place = jnp.zeros_like(rel)
+        for j, (dz, dx) in enumerate(OFFS):
+            place = jnp.where(rel == dz * 4 + dx, j, place)
+        places.append(place)
+        counts = counts + jnp.where(code == place, 1.0, 0.0)
+    earlier = lax.broadcasted_iota(jnp.int32, (TOK, TOK), 0) < lax.broadcasted_iota(
+        jnp.int32, (TOK, TOK), 1
+    )
+    before = jnp.dot(
+        counts.astype(BF16),
+        jnp.where(earlier, 1.0, 0.0).astype(BF16),
+        preferred_element_type=F32,
+    )
+    row = lax.broadcasted_iota(jnp.int32, (16 * PAD, TOK), 0)
+    disp, comb = jnp.zeros((16 * PAD, TOK), F32), jnp.zeros((16 * PAD, TOK), F32)
+    for k in range(2):
+        slot = jnp.sum(jnp.where(code == places[k], before, 0.0), axis=0, keepdims=True)
+        hit = row == places[k] * PAD + slot.astype(jnp.int32)
+        disp = jnp.where(hit, 1.0, disp)
+        comb = jnp.where(hit, rweights_ref[k : k + 1, :], comb)
+    disp_ref[...] = disp.astype(BF16)
+    comb = comb.T
+    high = comb.astype(BF16)
+    comb_ref[0] = high
+    comb_ref[1] = (comb - high.astype(F32)).astype(BF16)
+
+    for cp in ccopies:
+        cp.wait_recv()
+
+    @pl.when(tp == 0)
+    def _():
+        own_edge.wait_recv()
+
+    no_edge = jnp.logical_and(sp == 0, tp == 0)
+    keep = jnp.where(no_edge, 0.0, 1.0)
+    edge_mask = jnp.where(lax.broadcasted_iota(jnp.int32, (EDGE + TOK, TOK), 0) < EDGE, keep, 1.0)
+
+    def filtered(b, sums):
+        padf[...] = gbuf[b].astype(F32) * edge_mask
+        w = taps[b].astype(F32)
+        total = w[0:1] * padf[2 : 2 + TOK, :]
+        for k in range(1, 31):
+            total = total + w[k : k + 1] * padf[2 + k : 2 + k + TOK, :]
+        conv[b] = total
+        return sums[0] + total, sums[1] + total * total
+
+    zero = jnp.zeros((TOK, TOK), F32)
+    sum1, sum2 = lax.fori_loop(0, 8, filtered, (zero, zero))
+    mean = jnp.sum(sum1, axis=1, keepdims=True) / D_A
+    var = jnp.sum(sum2, axis=1, keepdims=True) / D_A - mean * mean
+    rstd = lax.rsqrt(var + 1e-05)
+
+    @pl.loop(0, 8)
+    def _(b):
+        w = taps[b].astype(F32)
+        v = (conv[b] - mean) * rstd * w[31:32] + w[32:33]
+        act[:, pl.ds(pl.multiple_of(b * TOK, TOK), TOK)] = (v * (1.0 / (1.0 + jnp.exp(-v)))).astype(
+            BF16
+        )
+
+    icopies[3].wait()
+
+    @pl.loop(0, 8)
+    def _(n):
+        cols = pl.ds(pl.multiple_of(n * 256, 256), 256)
+        branch[:, cols] = jnp.dot(act[...], proj[:, cols], preferred_element_type=F32).astype(BF16)
+
+    icopies[2].wait()
+
+    @pl.loop(0, 8)
+    def _(n):
+        rows = pl.ds(pl.multiple_of(n * 16, 16), 16)
+        b = branch[rows, :].astype(F32)
+        scale = lax.rsqrt(jnp.mean(b * b, axis=1, keepdims=True) + 1e-06)
+        st = resid[rows, :].astype(F32) + b * scale * gains_ref[0:1, :]
+        stream_ref[rows, :] = st
+        scale = lax.rsqrt(jnp.mean(st * st, axis=1, keepdims=True) + 1e-06)
+        normed_ref[rows, :] = (st * scale * gains_ref[1:2, :]).astype(BF16)
 
     acopies = {}
     for i in range(NG):
@@ -289,21 +462,40 @@
     mix = jnp.dot(comb_ref[0], ret, preferred_element_type=F32)
     mix = mix + jnp.dot(comb_ref[1], ret, preferred_element_type=F32)
     scale = lax.rsqrt(jnp.mean(mix * mix, axis=1, keepdims=True) + 1e-06)
-    out_ref[...] = (stream_ref[...] + mix * scale * gain_ref[...].astype(F32)).astype(BF16)
+    out_ref[...] = (stream_ref[...] + mix * scale * gains_ref[2:3, :]).astype(BF16)
     for cp in sends:
         cp.wait_send()
 
-
-def moe(normed, stream, disp, comb, gain, wg, wu, wd):
+    @pl.when(tp == 0)
+    def _():
+        own_edge.wait_send()
+
+
+def layer(*operands):
     vmem = pl.BlockSpec(memory_space=pltpu.VMEM)
     hbm = pl.BlockSpec(memory_space=pl.ANY)
     dma = pltpu.SemaphoreType.DMA
     return pl.pallas_call(
-        moe_kernel,
+        layer_kernel,
         out_shape=jax.ShapeDtypeStruct((TOK, D), BF16),
-        in_specs=[vmem] * 5 + [hbm] * 3,
+        in_specs=[hbm, hbm, vmem, hbm, hbm, vmem, vmem, vmem, hbm, hbm, hbm],
         out_specs=vmem,
         scratch_shapes=[
+            pltpu.VMEM((8 * TOK, TOK), BF16),
+            pltpu.VMEM((8 * TOK, TOK), BF16),
+            pltpu.VMEM((TOK, D), BF16),
+            pltpu.VMEM((D_A, D), BF16),
+            pltpu.VMEM((8 * TOK, TOK), BF16),
+            pltpu.VMEM((8, 48, TOK), BF16),
+            pltpu.VMEM((8, EDGE + TOK, TOK), BF16),
+            pltpu.VMEM((EDGE + TOK, TOK), F32),
+            pltpu.VMEM((8, TOK, TOK), F32),
+            pltpu.VMEM((TOK, D_A), BF16),
+            pltpu.VMEM((TOK, D), BF16),
+            pltpu.VMEM((TOK, D), F32),
+            pltpu.VMEM((TOK, D), BF16),
+            pltpu.VMEM((2, TOK, 16 * PAD), BF16),
+            pltpu.VMEM((16 * PAD, TOK), BF16),
             pltpu.VMEM((7, D, 256), BF16),
             pltpu.VMEM((FFB, D), BF16),
             pltpu.VMEM((16, PAD, D), BF16),
@@ -316,7 +508,10 @@
             pltpu.VMEM((NG, 2, ROWS, D), BF16),
             pltpu.VMEM((16, PAD, D), BF16),
             pltpu.VMEM((16, PAD, D), BF16),
+            dma((4,)),
             dma((15,)),
+            dma((22,)),
+            dma((22,)),
             dma((16,)),
             dma((16,)),
             dma((NG, 8)),
@@ -329,53 +524,8 @@
         compiler_params=pltpu.CompilerParams(
             collective_id=0, has_side_effects=True, vmem_limit_bytes=62 * 1024 * 1024
         ),
-        name="moe",
-    )(normed, stream, disp, comb, gain, wg, wu, wd)
-
-
-def passed_along(value, axis, steps):
-    count = lax.axis_size(axis)
-    leading, last = (max(0, -steps), min(count, count - steps))
-    return lax.ppermute(value, axis, [(source, source + steps) for source in range(leading, last)])
-
-
-def copy_for_each(value, axis):
-    copies = jnp.broadcast_to(value, (lax.axis_size(axis), *value.shape))
-    return lax.all_to_all(copies, axis, split_axis=0, concat_axis=0, tiled=True)
-
-
-def over_copies(value, axis):
-    return copy_for_each(value, axis).sum(axis=0)
-
-
-def together(arrays, axis):
-    ends = [0]
-    for a in arrays:
-        ends.append(ends[-1] + a.size)
-    subtotal = over_copies(jnp.concatenate([a.ravel() for a in arrays]), axis)
-    return tuple((subtotal[b:e].reshape(a.shape) for a, b, e in zip(arrays, ends, ends[1:])))
-
-
-def route_tables(routes, route_weights):
-    sp = lax.axis_index("sp")
-    z, x = sp // 4, sp % 4
-    flat = routes.reshape(-1)
-    experts = jnp.arange(16, dtype=jnp.int32)
-    matches = (flat[:, None] == experts[None, :]).astype(jnp.int32)
-    before = jnp.cumsum(matches, axis=0) - matches
-    slot = jnp.sum(before * matches, axis=1)
-    rel = ((flat // 4 - z) % 4) * 4 + (flat % 4 - x) % 4
-    place = jnp.zeros_like(rel)
-    for j, (dz, dx) in enumerate(OFFS):
-        place = place + jnp.where(rel == dz * 4 + dx, j, 0)
-    target = (place * PAD + slot).reshape(TOK, 2)
-    slots = jnp.arange(16 * PAD, dtype=jnp.int32)
-    disp = jnp.any(target.T[:, None, :] == slots[None, :, None], axis=0).astype(BF16)
-    hits = target[:, :, None] == slots[None, None, :]
-    comb = jnp.sum(jnp.where(hits, route_weights[:, :, None], 0.0), axis=1)
-    high = comb.astype(BF16)
-    low = (comb - high.astype(F32)).astype(BF16)
-    return disp, jnp.stack([high, low])
+        name="layer",
+    )(*operands)
 
 
 def per_device(
@@ -395,35 +545,22 @@
     down_weight,
     out_gain,
 ):
-    kernel_len = conv_weight.shape[0]
-    gated = (a_lin.astype(jnp.float32) * jax.nn.sigmoid(a_gate.astype(jnp.float32))).astype(
-        jnp.bfloat16
+    taps = jnp.concatenate(
+        [conv_weight, ln_gain[None, :], ln_bias[None, :], jnp.zeros((15, TOK), BF16)], axis=0
     )
-    row_count = gated.shape[0]
-    edge_rows = passed_along(gated[row_count - (kernel_len - 1) :], "sp", 1)
-    padded = jnp.concatenate([edge_rows, gated], 0).astype(jnp.float32)
-    filter_taps = conv_weight.astype(jnp.float32)
-    conv_out = filter_taps[0] * padded[0:row_count]
-    for offset in range(1, kernel_len):
-        conv_out = conv_out + filter_taps[offset] * padded[offset : offset + row_count]
-    row_total, squares = together(
-        (jnp.sum(conv_out, axis=1), jnp.sum(conv_out * conv_out, axis=1)), "tp"
-    )
-    row_mean = row_total / D_A
-    row_var = squares / D_A - row_mean * row_mean
-    scaled = (conv_out - row_mean[:, None]) * lax.rsqrt(row_var[:, None] + 1e-05)
-    scaled = scaled * ln_gain.astype(jnp.float32) + ln_bias.astype(jnp.float32)
-    activated = jax.nn.silu(scaled).astype(jnp.bfloat16)
-    token_acts = lax.all_to_all(activated, "tp", split_axis=0, concat_axis=1, tiled=True)
-    branch = jnp.dot(token_acts, proj_weight, preferred_element_type=jnp.float32)
-    branch_f = lax.optimization_barrier(branch.astype(jnp.bfloat16)).astype(jnp.float32)
-    branch_scale = lax.rsqrt(jnp.mean(branch_f * branch_f, axis=1, keepdims=True) + 1e-06)
-    stream = residual.astype(jnp.float32) + branch_f * branch_scale * mix_gain.astype(jnp.float32)
-    stream_scale = lax.rsqrt(jnp.mean(stream * stream, axis=1, keepdims=True) + 1e-06)
-    normed = (stream * stream_scale * ffn_gain.astype(jnp.float32)).astype(jnp.bfloat16)
-    disp, comb = route_tables(routes, route_weights)
-    return moe(
-        normed, stream, disp, comb, out_gain.reshape(1, D), gate_weight, up_weight, down_weight
+    gains = jnp.stack([mix_gain, ffn_gain, out_gain]).astype(F32)
+    return layer(
+        a_lin,
+        a_gate,
+        taps,
+        proj_weight,
+        residual,
+        gains,
+        routes.T,
+        route_weights.T,
+        gate_weight,
+        up_weight,
+        down_weight,
     )
 
 

time: 179 us -> 159 us (0.89); the launches traced: 179 us -> 156 us
  Pallas kernels: 137 us -> 150 us
  starting transfers between devices: 11.6 us -> 0 us
  waiting for transfers between devices: 10.7 us -> 0 us
  other arithmetic: 11.1 us -> 2.05 us
  matrix products: 2.94 us -> 0 us
    pallas_call x1, Pallas kernels: 137 us -> 150 us  [layer(): pl.pallas_call(layer_kernel, out_shape=jax.ShapeDtypeStruct((TOK, D), BF1...]
    all_to_all x2 -> x0, waiting for transfers between devices: 10.7 us -> none  [the longest x1 5.84 us: per_device(): lax.all_to_all(activated, 'tp', split_axis=0, concat_axis=1, tiled=True)]
    all_to_all x2 -> x0, starting transfers between devices: 8.06 us -> none  [the longest x1 4.47 us: copy_for_each(): return lax.all_to_all(copies, axis, split_axis=0, concat_axis=0, tiled=True)]
    convert_element_type x12 -> x1, other arithmetic: 4.79 us -> 0.65 us  [per_device(): gains = jnp.stack([mix_gain, ffn_gain, out_gain]).astype(F32)]
    reduce_sum x6 -> x0, other arithmetic: 3.96 us -> none  [the longest x1 2.38 us: per_device(): jnp.sum(conv_out, axis=1)]
    ppermute x1 -> x0, starting transfers between devices: 3.51 us -> none  [passed_along(): lax.ppermute(value, axis, [(source, source + steps) for source in range(l...]
    dot_general x1 -> x0, matrix products: 2.94 us -> none  [per_device(): jnp.dot(token_acts, proj_weight, preferred_element_type=jnp.float32)]
    another operation x1 -> x3, local copies, waits for them, and re-layouts: 0.01 us -> 2.08 us  [per_device(): gains = jnp.stack([mix_gain, ffn_gain, out_gain]).astype(F32)]
  transfers between devices with their start and end apart: 3 -> 0, of which waited for: 2 -> 0; matrix products, arithmetic and copies ran while one was open for 4% -> 0% of each run, Pallas kernels for 0% -> 0%
where the time goes in v2:
time: 159 us; the launch traced here: 156 us
  Pallas kernels  150 us (94%)
  local copies, waits for them, and re-layouts  4.04 us (3%)
  other arithmetic  2.05 us (1%)
    pallas_call x1, Pallas kernels, layer(): pl.pallas_call(layer_kernel, out_shape=jax.ShapeDtypeStruct((TOK, D), BF1...  150 us

profile of v2, /device:TPU:0, one launch (start us, length us, event | category | flops | bytes accessed | tf_op | source)
XLA Modules:
  0.0 156.4 jit_solution(5274185995668729481)
XLA Ops:
  0.0 0.1 pad.6.clone
  0.1 0.7 stack.12
  0.8 0.7 stack.13
  1.5 0.7 stack.14
  2.2 0.6 maximum_convert_fusion.gains_ref
  2.8 1.4 maximum_maximum_fusion.taps_ref
  4.2 150.3 %layer.1 = bf16[128,2048]{1,0:T(8,128)(2,1)} custom-call(bf16[1024,128]{1,0:T(8,128)(2,1)} %lin_hbm.1, bf16[1024,128]{1,0:T(8,128)(2,1)} %gate_hbm.1, bf16[48,128]{1,0:T(8,128)(2,1)} %maximum_maximum_fusion.taps_ref, bf16[1024,2048]{1,0:T(8,128)(2,1)} %proj_hbm.1, bf16[128,2048]{1,0:T(8,128)(2,1)} %resid_hbm.1, f32[3,2048]{1,0:T(4,128)} %maximum_convert_fusion.gains_ref, ...), custom_call_target="tpu_custom_call" | custom-call | tf_op jit(solution)/shard_map/layer/pallas_call | solution.py:478
  154.5 1.9 %copy.17 = bf16[128,2048]{1,0:T(8,128)(2,1)} copy(bf16[128,2048]{1,0:T(8,128)(2,1)} %layer.1) | data formatting | bytes 1048576
  (1 shorter events, 0.0 us)

commit v3 on v2

--- a/solution.py
+++ b/solution.py
@@ -13,6 +13,7 @@
 PAD = 24
 TOK = 128
 NG = 4
+DN = 1024
 ROWS = 4 * CAP
 PADROWS = 4 * PAD
 EDGE = 32
@@ -21,10 +22,10 @@
 F32 = jnp.float32
 
 GROUPS = (
-    ((0, 1), (0, 3), (1, 0), (3, 0)),
+    ((1, 1), (1, 3), (3, 1), (3, 3)),
     ((0, 0), (0, 2), (2, 0), (2, 2)),
     ((2, 1), (2, 3), (1, 2), (3, 2)),
-    ((1, 1), (1, 3), (3, 1), (3, 3)),
+    ((0, 1), (0, 3), (1, 0), (3, 0)),
 )
 OFFS = tuple(o for g in GROUPS for o in g)
 SELF = OFFS.index((0, 0))
@@ -33,10 +34,14 @@
 def layer_kernel(
     lin_hbm,
     gate_hbm,
-    taps_ref,
+    conv_ref,
+    lng_ref,
+    lnb_ref,
     proj_hbm,
     resid_hbm,
-    gains_ref,
+    mixg_ref,
+    ffng_ref,
+    outg_ref,
     routes_ref,
     rweights_ref,
     wg_hbm,
@@ -48,6 +53,7 @@
     resid,
     proj,
     gsrc,
+    small,
     taps,
     gbuf,
     padf,
@@ -101,9 +107,59 @@
             ((lin_hbm, lin), (gate_hbm, gatein), (resid_hbm, resid), (proj_hbm, proj))
         )
     ]
-    for cp in icopies:
+    icopies[0].start()
+    icopies[1].start()
+
+    barrier = pltpu.get_barrier_semaphore()
+
+    def greet(spi, tpi):
+        pl.semaphore_signal(
+            barrier, inc=1, device_id={"sp": spi, "tp": tpi}, device_id_type=MESH
+        )
+
+    for r in range(1, 8):
+        greet(sp, lax.rem(tp + r, 8))
+    for o in OFFS:
+        if o != (0, 0):
+            greet(sp_at(*o), tp)
+
+    @pl.when(tp == 0)
+    def _():
+        for t in range(1, 8):
+            greet(lax.rem(sp + 15, 16), t)
+
+    def remote(src, dst, ssem, rsem, spi, tpi):
+        return pltpu.make_async_remote_copy(
+            src_ref=src,
+            dst_ref=dst,
+            send_sem=ssem,
+            recv_sem=rsem,
+            device_id={"sp": spi, "tp": tpi},
+            device_id_type=MESH,
+        )
+
+    sends = []
+    ccopies = []
+
+    def exchange(n, src, dst, spi, tpi):
+        cp = remote(src, dst, c_s.at[n], c_r.at[n], spi, tpi)
         cp.start()
-
+        ccopies.append(cp)
+        sends.append(cp)
+
+    def edge_of(t):
+        return pl.ds(pl.multiple_of(lax.rem(t + 7, 8) * TOK + TOK - EDGE, EDGE), EDGE)
+
+    def body_of(t):
+        return pl.ds(pl.multiple_of(t * TOK, TOK), TOK)
+
+    small[...] = jnp.zeros((48, TOK), BF16)
+    small[0:31] = conv_ref[...]
+    small[31:32] = lng_ref[...].reshape(1, TOK)
+    small[32:33] = lnb_ref[...].reshape(1, TOK)
+    taps[tp] = small[...]
+    icopies[0].wait()
+    icopies[1].wait()
     wcopies = []
     for j in range(7):
         cols = pl.ds(128 * j, 128)
@@ -114,69 +170,29 @@
                 )
             )
     wcopies.append(pltpu.make_async_copy(wd_hbm.at[0], wd, wsem.at[14]))
-    for cp in wcopies:
+    for cp in icopies[2:] + wcopies:
         cp.start()
 
-    barrier = pltpu.get_barrier_semaphore()
-
-    def greet(spi, tpi):
-        pl.semaphore_signal(
-            barrier, inc=1, device_id={"sp": spi, "tp": tpi}, device_id_type=MESH
-        )
-
+
+    def gate(t):
+        g = gatein[body_of(t), :].astype(F32)
+        v = lin[body_of(t), :].astype(F32) * (1.0 / (1.0 + jnp.exp(-g)))
+        gsrc[body_of(t), :] = v.astype(BF16)
+
+    gate(tp)
+    gate(lax.rem(tp + 1, 8))
+    pl.semaphore_wait(barrier, 22 + jnp.minimum(tp, 1))
     for r in range(1, 8):
-        greet(sp, lax.rem(tp + r, 8))
-    for o in OFFS:
-        if o != (0, 0):
-            greet(sp_at(*o), tp)
-
-    @pl.when(tp == 0)
-    def _():
-        for t in range(1, 8):
-            greet(lax.rem(sp + 15, 16), t)
-
-    icopies[0].wait()
-    icopies[1].wait()
-    for n in range(4):
-        rows = pl.ds(256 * n, 256)
-        g = gatein[rows, :].astype(F32)
-        gsrc[rows, :] = (lin[rows, :].astype(F32) * (1.0 / (1.0 + jnp.exp(-g)))).astype(BF16)
-    pl.semaphore_wait(barrier, 22 + jnp.minimum(tp, 1))
-
-    def remote(src, dst, ssem, rsem, spi, tpi):
-        return pltpu.make_async_remote_copy(
-            src_ref=src,
-            dst_ref=dst,
-            send_sem=ssem,
-            recv_sem=rsem,
-            device_id={"sp": spi, "tp": tpi},
-            device_id_type=MESH,
-        )
-
-    sends = []
-    ccopies = []
-
-    def exchange(n, src, dst, spi, tpi):
-        cp = remote(src, dst, c_s.at[n], c_r.at[n], spi, tpi)
-        cp.start()
-        ccopies.append(cp)
-        sends.append(cp)
-
-    def edge_of(t):
-        return pl.ds(pl.multiple_of(lax.rem(t + 7, 8) * TOK + TOK - EDGE, EDGE), EDGE)
-
-    def body_of(t):
-        return pl.ds(pl.multiple_of(t * TOK, TOK), TOK)
-
+        exchange(13 + r, small, taps.at[tp], sp, lax.rem(tp + r, 8))
     for r in range(1, 8):
         t = lax.rem(tp + r, 8)
+        if r > 1:
+            gate(t)
         exchange(r - 1, gsrc.at[body_of(t)], gbuf.at[tp, pl.ds(EDGE, TOK)], sp, t)
         first = lax.div(8 - t, 8)
         exchange(
             6 + r, gsrc.at[edge_of(t)], gbuf.at[tp, pl.ds(0, EDGE)], lax.rem(sp + first, 16), t
         )
-    for r in range(1, 8):
-        exchange(13 + r, taps_ref, taps.at[tp], sp, lax.rem(tp + r, 8))
     own_edge = remote(
         gsrc.at[edge_of(0)],
         gbuf.at[tp, pl.ds(0, EDGE)],
@@ -195,7 +211,6 @@
         gbuf[tp, 0:EDGE] = gsrc[edge_of(tp), :]
 
     gbuf[tp, EDGE:] = gsrc[body_of(tp), :]
-    taps[tp] = taps_ref[...]
 
     lane = lax.broadcasted_iota(jnp.int32, (1, TOK), 1)
     code = lax.broadcasted_iota(jnp.int32, (16, TOK), 0)
@@ -266,22 +281,24 @@
 
     icopies[3].wait()
 
-    @pl.loop(0, 8)
+    @pl.loop(0, 2)
     def _(n):
-        cols = pl.ds(pl.multiple_of(n * 256, 256), 256)
+        cols = pl.ds(pl.multiple_of(n * 1024, 1024), 1024)
         branch[:, cols] = jnp.dot(act[...], proj[:, cols], preferred_element_type=F32).astype(BF16)
 
     icopies[2].wait()
-
-    @pl.loop(0, 8)
+    mixg = mixg_ref[...].astype(F32).reshape(1, D)
+    ffng = ffng_ref[...].astype(F32).reshape(1, D)
+
+    @pl.loop(0, 4)
     def _(n):
-        rows = pl.ds(pl.multiple_of(n * 16, 16), 16)
+        rows = pl.ds(pl.multiple_of(n * 32, 32), 32)
         b = branch[rows, :].astype(F32)
         scale = lax.rsqrt(jnp.mean(b * b, axis=1, keepdims=True) + 1e-06)
-        st = resid[rows, :].astype(F32) + b * scale * gains_ref[0:1, :]
+        st = resid[rows, :].astype(F32) + b * scale * mixg
         stream_ref[rows, :] = st
         scale = lax.rsqrt(jnp.mean(st * st, axis=1, keepdims=True) + 1e-06)
-        normed_ref[rows, :] = (st * scale * gains_ref[1:2, :]).astype(BF16)
+        normed_ref[rows, :] = (st * scale * ffng).astype(BF16)
 
     acopies = {}
     for i in range(NG):
@@ -356,7 +373,7 @@
         rs[i][n] = cp
         sends.append(cp)
 
-    def experts(i):
+    def hidden(i):
         if i == 0:
             for cp in wcopies[:14]:
                 cp.wait()
@@ -368,19 +385,20 @@
             h = g * (1.0 / (1.0 + jnp.exp(-g))) * u
             hbuf[:, pl.ds(pl.multiple_of(j * 128, 128), 128)] = h.astype(BF16)
 
+    def partial(i):
         if i == 0:
             wcopies[14].wait()
         for half in (1, 0):
 
-            @pl.loop(0, 8)
+            @pl.loop(0, D // DN)
             def _(n):
-                cols = pl.ds(pl.multiple_of(n * 256, 256), 256)
+                cols = pl.ds(pl.multiple_of(n * DN, DN), DN)
                 p = jnp.dot(
                     hbuf[4 * ROWS * half : 4 * ROWS * (half + 1), :],
                     wd[:, cols],
                     preferred_element_type=F32,
                 )
-                pbuf[i, half, :, :, cols] = p.astype(BF16).reshape(4, ROWS, 256)
+                pbuf[i, half, :, :, cols] = p.astype(BF16).reshape(4, ROWS, DN)
 
             if half == 1:
                 rs_copy(i, 0, pbuf.at[i, 1], precv.at[i], mate)
@@ -433,27 +451,31 @@
     gather1(2)
     gather2(1)
     gather3(0)
-    experts(0)
-    scatter1(0)
+    hidden(0)
+    partial(0)
     gather1(3)
     gather2(2)
+    scatter1(0)
+    gather3(1)
+    hidden(1)
     scatter2(0)
-    gather3(1)
-    experts(1)
+    gather2(3)
+    partial(1)
     scatter1(1)
-    gather2(3)
+    gather3(2)
+    hidden(2)
     scatter2(1)
-    gather3(2)
-    experts(2)
+    give_back(0)
+    partial(2)
     scatter1(2)
-    give_back(0)
+    gather3(3)
+    hidden(3)
     scatter2(2)
-    gather3(3)
-    experts(3)
+    give_back(1)
+    partial(3)
     scatter1(3)
-    give_back(1)
+    give_back(2)
     scatter2(3)
-    give_back(2)
     give_back(3)
     for j in range(16):
         if j != SELF:
@@ -462,7 +484,7 @@
     mix = jnp.dot(comb_ref[0], ret, preferred_element_type=F32)
     mix = mix + jnp.dot(comb_ref[1], ret, preferred_element_type=F32)
     scale = lax.rsqrt(jnp.mean(mix * mix, axis=1, keepdims=True) + 1e-06)
-    out_ref[...] = (stream_ref[...] + mix * scale * gains_ref[2:3, :]).astype(BF16)
+    out_ref[...] = (stream_ref[...] + mix * scale * outg_ref[...].astype(F32).reshape(1, D)).astype(BF16)
     for cp in sends:
         cp.wait_send()
 
@@ -478,7 +500,7 @@
     return pl.pallas_call(
         layer_kernel,
         out_shape=jax.ShapeDtypeStruct((TOK, D), BF16),
-        in_specs=[hbm, hbm, vmem, hbm, hbm, vmem, vmem, vmem, hbm, hbm, hbm],
+        in_specs=[hbm, hbm, vmem, vmem, vmem, hbm, hbm, vmem, vmem, vmem, vmem, vmem, hbm, hbm, hbm],
         out_specs=vmem,
         scratch_shapes=[
             pltpu.VMEM((8 * TOK, TOK), BF16),
@@ -486,6 +508,7 @@
             pltpu.VMEM((TOK, D), BF16),
             pltpu.VMEM((D_A, D), BF16),
             pltpu.VMEM((8 * TOK, TOK), BF16),
+            pltpu.VMEM((48, TOK), BF16),
             pltpu.VMEM((8, 48, TOK), BF16),
             pltpu.VMEM((8, EDGE + TOK, TOK), BF16),
             pltpu.VMEM((EDGE + TOK, TOK), F32),
@@ -545,17 +568,17 @@
     down_weight,
     out_gain,
 ):
-    taps = jnp.concatenate(
-        [conv_weight, ln_gain[None, :], ln_bias[None, :], jnp.zeros((15, TOK), BF16)], axis=0
-    )
-    gains = jnp.stack([mix_gain, ffn_gain, out_gain]).astype(F32)
     return layer(
         a_lin,
         a_gate,
-        taps,
+        conv_weight,
+        ln_gain,
+        ln_bias,
         proj_weight,
         residual,
-        gains,
+        mix_gain,
+        ffn_gain,
+        out_gain,
         routes.T,
         route_weights.T,
         gate_weight,

time: 159 us -> 135 us (0.85); the launches traced: 156 us -> 135 us
  Pallas kernels: 150 us -> 133 us
  local copies, waits for them, and re-layouts: 4.04 us -> 1.88 us
  other arithmetic: 2.05 us -> 0 us
    pallas_call x1, Pallas kernels: 150 us -> 133 us  [layer(): pl.pallas_call(layer_kernel, out_shape=jax.ShapeDtypeStruct((TOK, D), BF1...]
    another operation x3 -> x0, local copies, waits for them, and re-layouts: 2.08 us -> none  [per_device(): gains = jnp.stack([mix_gain, ffn_gain, out_gain]).astype(F32)]
where the time goes in v3:
time: 135 us
  Pallas kernels  133 us (99%)
  local copies, waits for them, and re-layouts  1.88 us (1%)
    pallas_call x1, Pallas kernels, layer(): pl.pallas_call(layer_kernel, out_shape=jax.ShapeDtypeStruct((TOK, D), BF1...  133 us

profile of v3, /device:TPU:0, one launch (start us, length us, event | category | flops | bytes accessed | tf_op | source)
XLA Modules:
  0.0 134.9 jit_solution(7211345951031620274)
XLA Ops:
  0.0 133.0 %layer.1 = bf16[128,2048]{1,0:T(8,128)(2,1)} custom-call(bf16[1024,128]{1,0:T(8,128)(2,1)} %lin_hbm.1, bf16[1024,128]{1,0:T(8,128)(2,1)} %gate_hbm.1, bf16[31,128]{1,0:T(8,128)(2,1)} %conv_ref.1, bf16[128]{0:T(256)(128)(2,1)} %lng_ref.1, bf16[128]{0:T(256)(128)(2,1)} %lnb_ref.1, bf16[1024,2048]{1,0:T(8,128)(2,1)} %proj_hbm.1, bf16[128,2048]{1,0:T(8,128)(2,1)} %resid_hbm.1, ...), custom_call_target="tpu_custom_call" | custom-call | tf_op jit(solution)/shard_map/layer/pallas_call | solution.py:500
  133.0 1.9 %copy.17 = bf16[128,2048]{1,0:T(8,128)(2,1)} copy(bf16[128,2048]{1,0:T(8,128)(2,1)} %layer.1) | data formatting | bytes 1048576

commit v4 on v3

--- a/solution.py
+++ b/solution.py
@@ -13,19 +13,19 @@
 PAD = 24
 TOK = 128
 NG = 4
-DN = 1024
 ROWS = 4 * CAP
 PADROWS = 4 * PAD
 EDGE = 32
+EARLY = 16
 MESH = pl.DeviceIdType.MESH
 BF16 = jnp.bfloat16
 F32 = jnp.float32
 
 GROUPS = (
-    ((1, 1), (1, 3), (3, 1), (3, 3)),
+    ((0, 1), (0, 3), (1, 0), (3, 0)),
+    ((1, 1), (3, 3), (3, 1), (1, 3)),
+    ((2, 1), (2, 3), (1, 2), (3, 2)),
     ((0, 0), (0, 2), (2, 0), (2, 2)),
-    ((2, 1), (2, 3), (1, 2), (3, 2)),
-    ((0, 1), (0, 3), (1, 0), (3, 0)),
 )
 OFFS = tuple(o for g in GROUPS for o in g)
 SELF = OFFS.index((0, 0))
@@ -63,6 +63,7 @@
     stream_ref,
     normed_ref,
     comb_ref,
+    mixed,
     disp_ref,
     wgu,
     wd,
@@ -139,12 +140,12 @@
         )
 
     sends = []
-    ccopies = []
+    ccopies = {}
 
     def exchange(n, src, dst, spi, tpi):
         cp = remote(src, dst, c_s.at[n], c_r.at[n], spi, tpi)
         cp.start()
-        ccopies.append(cp)
+        ccopies[n] = cp
         sends.append(cp)
 
     def edge_of(t):
@@ -153,7 +154,7 @@
     def body_of(t):
         return pl.ds(pl.multiple_of(t * TOK, TOK), TOK)
 
-    small[...] = jnp.zeros((48, TOK), BF16)
+    small[...] = jnp.zeros((40, TOK), BF16)
     small[0:31] = conv_ref[...]
     small[31:32] = lng_ref[...].reshape(1, TOK)
     small[32:33] = lnb_ref[...].reshape(1, TOK)
@@ -175,23 +176,26 @@
 
 
     def gate(t):
-        g = gatein[body_of(t), :].astype(F32)
-        v = lin[body_of(t), :].astype(F32) * (1.0 / (1.0 + jnp.exp(-g)))
-        gsrc[body_of(t), :] = v.astype(BF16)
-
-    gate(tp)
-    gate(lax.rem(tp + 1, 8))
+        rows = pl.ds(TOK * t, TOK)
+        g = gatein[rows, :].astype(F32)
+        v = lin[rows, :].astype(F32) * (1.0 / (1.0 + jnp.exp(-g)))
+        gsrc[rows, :] = v.astype(BF16)
+
+    for r in range(8):
+        gate(r)
     pl.semaphore_wait(barrier, 22 + jnp.minimum(tp, 1))
-    for r in range(1, 8):
-        exchange(13 + r, small, taps.at[tp], sp, lax.rem(tp + r, 8))
-    for r in range(1, 8):
-        t = lax.rem(tp + r, 8)
-        if r > 1:
-            gate(t)
-        exchange(r - 1, gsrc.at[body_of(t)], gbuf.at[tp, pl.ds(EDGE, TOK)], sp, t)
+    peers = [(dy, o) for dy in range(4) for o in range(2)][1:]
+
+    def peer(dy, o):
+        return lax.rem(y + dy, 4) * 2 + (c if o == 0 else 1 - c)
+
+    for n, p in enumerate(peers):
+        t = peer(*p)
+        exchange(14 + n, small, taps.at[tp], sp, t)
+        exchange(n, gsrc.at[body_of(t)], gbuf.at[tp, pl.ds(EDGE, TOK)], sp, t)
         first = lax.div(8 - t, 8)
         exchange(
-            6 + r, gsrc.at[edge_of(t)], gbuf.at[tp, pl.ds(0, EDGE)], lax.rem(sp + first, 16), t
+            7 + n, gsrc.at[edge_of(t)], gbuf.at[tp, pl.ds(0, EDGE)], lax.rem(sp + first, 16), t
         )
     own_edge = remote(
         gsrc.at[edge_of(0)],
@@ -242,31 +246,40 @@
     disp_ref[...] = disp.astype(BF16)
     comb = comb.T
     high = comb.astype(BF16)
-    comb_ref[0] = high
-    comb_ref[1] = (comb - high.astype(F32)).astype(BF16)
-
-    for cp in ccopies:
-        cp.wait_recv()
-
-    @pl.when(tp == 0)
-    def _():
-        own_edge.wait_recv()
+    low = (comb - high.astype(F32)).astype(BF16)
+    for i in range(NG):
+        comb_ref[0, i] = high[:, PADROWS * i : PADROWS * (i + 1)]
+        comb_ref[1, i] = low[:, PADROWS * i : PADROWS * (i + 1)]
 
     no_edge = jnp.logical_and(sp == 0, tp == 0)
     keep = jnp.where(no_edge, 0.0, 1.0)
     edge_mask = jnp.where(lax.broadcasted_iota(jnp.int32, (EDGE + TOK, TOK), 0) < EDGE, keep, 1.0)
 
-    def filtered(b, sums):
+    def filtered(b):
         padf[...] = gbuf[b].astype(F32) * edge_mask
         w = taps[b].astype(F32)
         total = w[0:1] * padf[2 : 2 + TOK, :]
         for k in range(1, 31):
             total = total + w[k : k + 1] * padf[2 + k : 2 + k + TOK, :]
         conv[b] = total
-        return sums[0] + total, sums[1] + total * total
-
-    zero = jnp.zeros((TOK, TOK), F32)
-    sum1, sum2 = lax.fori_loop(0, 8, filtered, (zero, zero))
+        return total, total * total
+
+    def arrived(n):
+        for k in (n, 7 + n, 14 + n):
+            ccopies[k].wait_recv()
+        dy, o = peers[n]
+        return peer((4 - dy) % 4, o)
+
+    sum1, sum2 = filtered(arrived(0))
+    for n in range(1, 8):
+        if n == 7:
+
+            @pl.when(tp == 0)
+            def _():
+                own_edge.wait_recv()
+
+        more1, more2 = filtered(tp) if n == 7 else filtered(arrived(n))
+        sum1, sum2 = sum1 + more1, sum2 + more2
     mean = jnp.sum(sum1, axis=1, keepdims=True) / D_A
     var = jnp.sum(sum2, axis=1, keepdims=True) / D_A - mean * mean
     rstd = lax.rsqrt(var + 1e-05)
@@ -300,7 +313,25 @@
         scale = lax.rsqrt(jnp.mean(st * st, axis=1, keepdims=True) + 1e-06)
         normed_ref[rows, :] = (st * scale * ffng).astype(BF16)
 
+    ag = [dict() for _ in range(NG)]
+
+    def ag_copy(i, n, src, dst, tpi):
+        cp = remote(src, dst, g_s.at[i, n], g_r.at[i, n], sp, tpi)
+        cp.start()
+        ag[i][n] = cp
+        sends.append(cp)
+
     acopies = {}
+
+    def dispatch(i):
+        for j in range(4 * i, 4 * i + 4):
+            if j != SELF:
+                acopies[j] = remote(
+                    outg.at[j], arecv.at[j], a_s.at[j], a_r.at[j], sp_at(*OFFS[j]), tp
+                )
+                acopies[j].start()
+                sends.append(acopies[j])
+
     for i in range(NG):
         rows = jnp.dot(
             disp_ref[PADROWS * i : PADROWS * (i + 1), :],
@@ -308,13 +339,13 @@
             preferred_element_type=F32,
         )
         outg[4 * i : 4 * i + 4] = rows.astype(BF16).reshape(4, PAD, D)
-        for j in range(4 * i, 4 * i + 4):
-            if j != SELF:
-                acopies[j] = remote(
-                    outg.at[j], arecv.at[j], a_s.at[j], a_r.at[j], sp_at(*OFFS[j]), tp
-                )
-                acopies[j].start()
-                sends.append(acopies[j])
+        if i == SELF // 4:
+            xbuf[i, 0, 0, 0:EARLY] = outg[SELF, 0:EARLY]
+            early = pl.ds(0, EARLY)
+            ag_copy(i, 8, xbuf.at[i, 0, 0, early], xbuf.at[i, 0, 3, early], up)
+            ag_copy(i, 9, xbuf.at[i, 0, 0, early], xbuf.at[i, 0, 1, early], down)
+        if i == 0:
+            dispatch(0)
 
     r_i = lax.broadcasted_iota(jnp.int32, (ROWS, PADROWS), 0)
     c_i = lax.broadcasted_iota(jnp.int32, (ROWS, PADROWS), 1)
@@ -324,14 +355,6 @@
     c_e = lax.broadcasted_iota(jnp.int32, (PADROWS, ROWS), 1)
     q_e = sum((c_e >= CAP * k).astype(jnp.int32) for k in (1, 2, 3))
     expand = (r_e == c_e + (PAD - CAP) * q_e).astype(F32).astype(BF16)
-
-    ag = [dict() for _ in range(NG)]
-
-    def ag_copy(i, n, src, dst, tpi):
-        cp = remote(src, dst, g_s.at[i, n], g_r.at[i, n], sp, tpi)
-        cp.start()
-        ag[i][n] = cp
-        sends.append(cp)
 
     def gather1(i):
         blocks = []
@@ -342,26 +365,34 @@
                 acopies[j].wait_recv()
                 blocks.append(arecv[j])
         own = jnp.dot(compact, jnp.concatenate(blocks, axis=0), preferred_element_type=F32)
-        xbuf[i, 0, 0] = own.astype(BF16)
-        src = xbuf.at[i, 0, 0]
-        ag_copy(i, 0, src, xbuf.at[i, 0, 3], up)
-        ag_copy(i, 1, src, xbuf.at[i, 0, 1], down)
-        ag_copy(i, 2, src, xbuf.at[i, 1, 0], mate)
+        start = EARLY if i == SELF // 4 else 0
+        rest = pl.ds(start, ROWS - start)
+        xbuf[i, 0, 0, start:] = own.astype(BF16)[start:]
+        src = xbuf.at[i, 0, 0, rest]
+        ag_copy(i, 0, src, xbuf.at[i, 0, 3, rest], up)
+        ag_copy(i, 1, src, xbuf.at[i, 0, 1, rest], down)
+        ag_copy(i, 2, xbuf.at[i, 0, 0], xbuf.at[i, 1, 0], mate)
 
     lo, hi = pl.ds(0, HALF), pl.ds(HALF, HALF)
 
     def gather2(i):
         ag[i][0].wait_recv()
+        if i == SELF // 4:
+            ag[i][8].wait_recv()
         ag_copy(i, 3, xbuf.at[i, 0, 3, :, lo], xbuf.at[i, 0, 2, :, lo], up)
         ag_copy(i, 6, xbuf.at[i, 0, 3], xbuf.at[i, 1, 3], mate)
         ag[i][1].wait_recv()
+        if i == SELF // 4:
+            ag[i][9].wait_recv()
         ag_copy(i, 4, xbuf.at[i, 0, 1, :, hi], xbuf.at[i, 0, 2, :, hi], down)
         ag_copy(i, 5, xbuf.at[i, 0, 1], xbuf.at[i, 1, 1], mate)
 
-    def gather3(i):
+    def relay(i):
         ag[i][3].wait_recv()
         ag[i][4].wait_recv()
         ag_copy(i, 7, xbuf.at[i, 0, 2], xbuf.at[i, 1, 2], mate)
+
+    def ready(i):
         for n in (2, 5, 6, 7):
             ag[i][n].wait_recv()
 
@@ -389,27 +420,26 @@
         if i == 0:
             wcopies[14].wait()
         for half in (1, 0):
-
-            @pl.loop(0, D // DN)
-            def _(n):
-                cols = pl.ds(pl.multiple_of(n * DN, DN), DN)
+            for cols in (lo, hi):
                 p = jnp.dot(
                     hbuf[4 * ROWS * half : 4 * ROWS * (half + 1), :],
                     wd[:, cols],
                     preferred_element_type=F32,
                 )
-                pbuf[i, half, :, :, cols] = p.astype(BF16).reshape(4, ROWS, DN)
-
-            if half == 1:
-                rs_copy(i, 0, pbuf.at[i, 1], precv.at[i], mate)
+                pbuf[i, half, :, :, cols] = p.astype(BF16).reshape(4, ROWS, HALF)
+                if half == 1:
+                    n = 0 if cols is lo else 7
+                    rs_copy(i, n, pbuf.at[i, 1, :, :, cols], precv.at[i, :, :, cols], mate)
 
     def both(i, k, cols):
         return pbuf[i, 0, k, :, cols].astype(F32) + precv[i, k, :, cols].astype(F32)
 
     def scatter1(i):
         rs[i][0].wait_recv()
-        pbuf[i, 0, 2] = both(i, 2, slice(None)).astype(BF16)
+        pbuf[i, 0, 2, :, :HALF] = both(i, 2, slice(0, HALF)).astype(BF16)
         rs_copy(i, 1, pbuf.at[i, 0, 2, :, lo], r1.at[i, 0], up)
+        rs[i][7].wait_recv()
+        pbuf[i, 0, 2, :, HALF:] = both(i, 2, slice(HALF, D)).astype(BF16)
         rs_copy(i, 2, pbuf.at[i, 0, 2, :, hi], r1.at[i, 1], down)
         pbuf[i, 0, 1, :, HALF:] = both(i, 1, slice(HALF, D)).astype(BF16)
         rs_copy(i, 3, pbuf.at[i, 0, 1, :, hi], r2.at[i, 0, :, hi], up)
@@ -446,29 +476,36 @@
                 sends.append(tcopies[j])
 
     gather1(0)
+    dispatch(1)
     gather1(1)
+    dispatch(2)
     gather2(0)
     gather1(2)
+    dispatch(3)
     gather2(1)
-    gather3(0)
+    relay(0)
+    ready(0)
     hidden(0)
-    partial(0)
     gather1(3)
     gather2(2)
+    relay(1)
+    partial(0)
+    ready(1)
     scatter1(0)
-    gather3(1)
     hidden(1)
+    gather2(3)
     scatter2(0)
-    gather2(3)
+    relay(2)
     partial(1)
+    ready(2)
     scatter1(1)
-    gather3(2)
     hidden(2)
     scatter2(1)
+    relay(3)
     give_back(0)
     partial(2)
+    ready(3)
     scatter1(2)
-    gather3(3)
     hidden(3)
     scatter2(2)
     give_back(1)
@@ -477,14 +514,19 @@
     give_back(2)
     scatter2(3)
     give_back(3)
-    for j in range(16):
-        if j != SELF:
-            tcopies[j].wait_recv()
-    ret = ret_r[...].reshape(16 * PAD, D)
-    mix = jnp.dot(comb_ref[0], ret, preferred_element_type=F32)
-    mix = mix + jnp.dot(comb_ref[1], ret, preferred_element_type=F32)
+    for i in range(NG):
+        if i == NG - 1:
+            mixed[...] = mix
+        for j in range(4 * i, 4 * i + 4):
+            if j != SELF:
+                tcopies[j].wait_recv()
+        ret = ret_r[4 * i : 4 * i + 4].reshape(PADROWS, D)
+        part = jnp.dot(comb_ref[0, i], ret, preferred_element_type=F32)
+        part = part + jnp.dot(comb_ref[1, i], ret, preferred_element_type=F32)
+        mix = part if i == 0 else mix + part if i < NG - 1 else mixed[...] + part
     scale = lax.rsqrt(jnp.mean(mix * mix, axis=1, keepdims=True) + 1e-06)
-    out_ref[...] = (stream_ref[...] + mix * scale * outg_ref[...].astype(F32).reshape(1, D)).astype(BF16)
+    result = stream_ref[...] + mix * scale * outg_ref[...].astype(F32).reshape(1, D)
+    out_ref[...] = result.astype(BF16)
     for cp in sends:
         cp.wait_send()
 
@@ -508,8 +550,8 @@
             pltpu.VMEM((TOK, D), BF16),
             pltpu.VMEM((D_A, D), BF16),
             pltpu.VMEM((8 * TOK, TOK), BF16),
-            pltpu.VMEM((48, TOK), BF16),
-            pltpu.VMEM((8, 48, TOK), BF16),
+            pltpu.VMEM((40, TOK), BF16),
+            pltpu.VMEM((8, 40, TOK), BF16),
             pltpu.VMEM((8, EDGE + TOK, TOK), BF16),
             pltpu.VMEM((EDGE + TOK, TOK), F32),
             pltpu.VMEM((8, TOK, TOK), F32),
@@ -517,7 +559,8 @@
             pltpu.VMEM((TOK, D), BF16),
             pltpu.VMEM((TOK, D), F32),
             pltpu.VMEM((TOK, D), BF16),
-            pltpu.VMEM((2, TOK, 16 * PAD), BF16),
+            pltpu.VMEM((2, NG, TOK, PADROWS), BF16),
+            pltpu.VMEM((TOK, D), F32),
             pltpu.VMEM((16 * PAD, TOK), BF16),
             pltpu.VMEM((7, D, 256), BF16),
             pltpu.VMEM((FFB, D), BF16),
@@ -537,10 +580,10 @@
             dma((22,)),
             dma((16,)),
             dma((16,)),
+            dma((NG, 10)),
+            dma((NG, 10)),
             dma((NG, 8)),
             dma((NG, 8)),
-            dma((NG, 7)),
-            dma((NG, 7)),
             dma((16,)),
             dma((16,)),
         ],

time: 135 us -> 122 us (0.904)
  Pallas kernels: 133 us -> 120 us
    pallas_call x1, Pallas kernels: 133 us -> 120 us  [layer(): pl.pallas_call(layer_kernel, out_shape=jax.ShapeDtypeStruct((TOK, D), BF1...]
where the time goes in v4:
time: 122 us
  Pallas kernels  120 us (98%)
  local copies, waits for them, and re-layouts  1.88 us (2%)
    pallas_call x1, Pallas kernels, layer(): pl.pallas_call(layer_kernel, out_shape=jax.ShapeDtypeStruct((TOK, D), BF1...  120 us

profile of v4, /device:TPU:0, one launch (start us, length us, event | category | flops | bytes accessed | tf_op | source)
XLA Modules:
  0.0 121.9 jit_solution(2553956446476856907)
XLA Ops:
  0.0 120.0 %layer.1 = bf16[128,2048]{1,0:T(8,128)(2,1)} custom-call(bf16[1024,128]{1,0:T(8,128)(2,1)} %lin_hbm.1, bf16[1024,128]{1,0:T(8,128)(2,1)} %gate_hbm.1, bf16[31,128]{1,0:T(8,128)(2,1)} %conv_ref.1, bf16[128]{0:T(256)(128)(2,1)} %lng_ref.1, bf16[128]{0:T(256)(128)(2,1)} %lnb_ref.1, bf16[1024,2048]{1,0:T(8,128)(2,1)} %proj_hbm.1, bf16[128,2048]{1,0:T(8,128)(2,1)} %resid_hbm.1, ...), custom_call_target="tpu_custom_call" | custom-call | tf_op jit(solution)/shard_map/layer/pallas_call | solution.py:542
  120.1 1.9 %copy.17 = bf16[128,2048]{1,0:T(8,128)(2,1)} copy(bf16[128,2048]{1,0:T(8,128)(2,1)} %layer.1) | data formatting | bytes 1048576
